TPU v7x, 32 devices: a whole 2x2x4 slice. The times are simulated.
32 devices in a mesh: sp: 8 (over z, x), tp: 4 (over y, core).
Axes of the slice: x: 2, y: 2, z: 4, core: 2. Of those that a mesh axis runs over, the one named last changes fastest.
Arguments:
- tokens: bfloat16 [6144, 2048], P(('sp', 'tp')), may hold values from -6 to 6
- in_gain: float32 [2048], replicated, may hold values from 0.1 to 1.9
- w_query: bfloat16 [2048, 1024], P(None, 'tp'), may hold values from -0.125 to 0.125
- w_key: bfloat16 [2048, 1024], P(None, 'tp'), may hold values from -0.125 to 0.125
- w_value: bfloat16 [2048, 2048], P(None, 'tp'), may hold values from -0.125 to 0.125
- w_input_gate: bfloat16 [2048, 8], replicated, may hold values from -8 to 8
- w_forget_gate: bfloat16 [2048, 8], replicated, may hold values from -0.125 to 0.125
- forget_bias: float32 [8], replicated
- forget_extra: float32 [6144, 8], P('sp', 'tp'), may hold values from -2 to 0
- w_conv_gate: bfloat16 [2048, 2048], P(None, 'tp'), may hold values from -0.125 to 0.125
- w_conv_left: bfloat16 [2048, 2048], P(None, 'tp'), may hold values from -0.125 to 0.125
- w_conv_right: bfloat16 [2048, 2048], P(None, 'tp'), may hold values from -0.125 to 0.125
- conv_taps: float32 [3, 2048], replicated, may hold values from -3.5 to 3.5
- first_memory: float32 [8, 128, 256], P('tp'), may hold values from -2560 to 2560
- first_norm: float32 [8, 128], P('tp'), may hold values from -2560 to 2560
- w_out_memory: bfloat16 [2048, 2048], P('tp'), may hold values from -0.09375 to 0.09375
- w_out_conv: bfloat16 [2048, 2048], P('tp'), may hold values from -0.09375 to 0.09375
Outputs:
- mixed: bfloat16 [6144, 2048], P(('sp', 'tp'))
All inputs are finite; a program needn't handle non-finite values.
Results may differ from a plain program's by a relative error of at most 0.015.
The roundings to bfloat16 on the way count: a program that leaves them out, or rounds other values in their place, can miss the bound.
Values may be sent and summed in bfloat16 or wider, within the bound.
A program may use at most 64 MiB of HBM per device.

v0:
```python
import functools

import jax
import jax.numpy as jnp
from jax import lax
from jax.experimental import pallas as pl
from jax.experimental.pallas import tpu as pltpu
from jax.sharding import PartitionSpec as P

KEY_DIM = 128
VALUE_DIM = 256
TAPS = 3
EPS = 1e-06
NEG = -1e30
MESH = pl.DeviceIdType.MESH
F32 = jnp.float32
BF16 = jnp.bfloat16
AG_CHUNKS = 6
RS_CHUNKS = 8


def mm(a, b):
    return lax.dot_general(a, b, (((1,), (0,)), ((), ())), preferred_element_type=F32)


def mm_t(a, b):
    return lax.dot_general(a, b, (((1,), (1,)), ((), ())), preferred_element_type=F32)


def scan_steps(n):
    steps, d = [], 1
    while d < n:
        steps.append(d)
        d *= 2
    return steps


def kernel(
    n_sp, n_tp, heads, channels, width,
    tokens, gain, wk, wv, wq, wcg, wcl, wcr, wig, wfg, bias, extra, taps, first_mem, first_norm,
    wom, woc, out,
    W, WO, XG, PJ, G, COL, NUM, DEN, HC, PROD, halo_out, halo_in,
    A_mem, E_mem, sm_out, sm_in, mem_out_b, mem_in_b, sq_out, sq_in,
    PS, DR, YS, YR,
    w_sem, ag_d, ag_ys, ag_yr, ag_fs, ag_fr, st_s, st_r, hl_s, sq_s, sq_r,
    rd_s, rd_r, ry_s, ry_r,
):
    sp = lax.axis_index("sp")
    tp = lax.axis_index("tp")
    core = lax.rem(tp, 2)
    y = tp // 2
    n_y = n_tp // 2
    partner = tp + 1 - 2 * core
    R, D = tokens.shape
    T = R * n_tp
    qk, vw = heads * KEY_DIM, heads * VALUE_DIM
    o_v, o_g = qk, qk + vw
    o_q = o_g + 128
    o_c = o_q + qk
    total = o_c + 3 * channels
    steps = scan_steps(n_sp)

    srcs = [(wk, 0, qk), (wv, o_v, vw), (wq, o_q, qk), (wcg, o_c, channels),
            (wcl, o_c + channels, channels), (wcr, o_c + 2 * channels, channels)]
    w_copies = [
        pltpu.make_async_copy(s, W.at[:, pl.ds(o, n)], w_sem.at[i])
        for i, (s, o, n) in enumerate(srcs)
    ]
    w_copies.append(pltpu.make_async_copy(wom, WO.at[pl.ds(0, vw), :], w_sem.at[6]))
    w_copies.append(pltpu.make_async_copy(woc, WO.at[pl.ds(vw, channels), :], w_sem.at[7]))
    for c in w_copies:
        c.start()

    def rows_of(block, count=1, first=0, n=None):
        n = R * count if n is None else n
        return pl.ds(pl.multiple_of(block * R + first, 16), n)

    def remote(src, dst, ss, rs, to_tp=None, to_sp=None):
        return pltpu.make_async_remote_copy(
            src_ref=src, dst_ref=dst, send_sem=ss, recv_sem=rs,
            device_id=(sp if to_sp is None else to_sp, tp if to_tp is None else to_tp),
            device_id_type=MESH,
        )

    offsets = sorted({d % n_sp for d in steps} | {(n_sp - d) % n_sp for d in steps})
    barrier = pltpu.get_barrier_semaphore()
    for k in range(1, n_tp):
        pl.semaphore_signal(barrier, inc=1, device_id=(sp, lax.rem(tp + k, n_tp)), device_id_type=MESH)
    for k in offsets:
        pl.semaphore_signal(barrier, inc=1, device_id=(lax.rem(sp + k, n_sp), tp), device_id_type=MESH)
    x = tokens[...].astype(F32)
    scale = lax.rsqrt(jnp.mean(x * x, axis=1, keepdims=True) + EPS)
    XG[rows_of(tp), :] = (x * scale * gain[...]).astype(BF16)
    pl.semaphore_wait(barrier, n_tp - 1 + len(offsets))

    sends = []
    piece = R // AG_CHUNKS
    for c in range(AG_CHUNKS):
        for k in range(1, n_y):
            r = rows_of(tp, 1, c * piece, piece)
            cp = remote(XG.at[r, :], XG.at[r, :], ag_ys.at[k - 1, c], ag_yr.at[k - 1, c],
                        to_tp=lax.rem(y + k, n_y) * 2 + core)
            cp.start()
            sends.append(cp)
    own = remote(XG.at[rows_of(tp), :], XG.at[rows_of(tp), :], ag_d.at[0], ag_d.at[1], to_tp=partner)
    own.start()

    tn = 256 if (o_g % 256 == 0 and qk % 256 == 0) else 128

    def project(block, first, last):
        rr = rows_of(block, 2)

        def one(j, _):
            cols = pl.ds(pl.multiple_of(first + j * tn, 128), tn)
            PJ[rr, cols] = mm(XG[rr, :], W[:, cols]).astype(BF16)
            return 0

        lax.fori_loop(0, (last - first) // tn, one, 0)

    def project_gates(block):
        rr = rows_of(block, 2)
        G[rr, :] = mm(XG[rr, :], W[:, o_g:o_g + 128])

    n_heads = bias.shape[0]
    W[:, o_g:o_g + 128] = jnp.concatenate(
        [wig[...].astype(F32), wfg[...].astype(F32), jnp.zeros((128 - 2 * n_heads, D), F32)],
        axis=0).T.astype(BF16)
    own.wait_recv()
    for c in w_copies[:2]:
        c.wait()
    project(2 * y, 0, o_g)
    project_gates(2 * y)
    for c in w_copies[2:6]:
        c.wait()
    project(2 * y, o_q, total)
    fwd = []
    for c in range(AG_CHUNKS):
        for k in range(1, n_y):
            src = lax.rem(y + n_y - k, n_y) * 2
            r = rows_of(src + core, 1, c * piece, piece)
            remote(XG.at[r, :], XG.at[r, :], ag_ys.at[k - 1, c], ag_yr.at[k - 1, c], to_tp=partner).wait_recv()
            cp = remote(XG.at[r, :], XG.at[r, :], ag_fs.at[k - 1, c], ag_fr.at[k - 1, c], to_tp=partner)
            cp.start()
            sends.append(cp)
    for c in range(AG_CHUNKS):
        for k in range(1, n_y):
            src = lax.rem(y + n_y - k, n_y) * 2
            r = rows_of(src + 1 - core, 1, c * piece, piece)
            remote(XG.at[r, :], XG.at[r, :], ag_fs.at[k - 1, c], ag_fr.at[k - 1, c], to_tp=partner).wait_recv()
    others = [lax.rem(y + k, n_y) * 2 for k in range(1, n_y)]
    for b in others:
        project(b, 0, o_g)
        project_gates(b)

    gt = G[...].T
    in_all, forget_all = gt[0:n_heads], gt[n_heads:2 * n_heads]
    sub = lax.broadcasted_iota(jnp.int32, (n_heads, T), 0)
    sub8 = lax.broadcasted_iota(jnp.int32, (8, T), 0)
    lane = lax.broadcasted_iota(jnp.int32, (8, T), 1)
    in_pre = jnp.zeros((8, T), F32)
    log_f = jnp.zeros((8, T), F32)
    for h in range(heads):
        head = tp * heads + h
        row_i = jnp.sum(jnp.where(sub == head, in_all, 0.0), axis=0, keepdims=True)
        row_f = jnp.sum(jnp.where(sub == head, forget_all, 0.0), axis=0, keepdims=True) + bias[head]
        row_f = jnp.minimum(row_f, 0.0) - jnp.log1p(jnp.exp(-jnp.abs(row_f))) + extra[h:h + 1, :]
        in_pre = jnp.where(sub8 == h, row_i, in_pre)
        log_f = jnp.where(sub8 == h, row_f, log_f)
    cum = log_f
    for d in scan_steps(T):
        cum = cum + jnp.where(lane >= d, pltpu.roll(cum, d, 1), 0.0)
    gap = in_pre - cum
    decay = cum[:, T - 1:T]
    gmax = jnp.max(gap, axis=1, keepdims=True)
    COL[...] = jnp.concatenate([jnp.exp(gap - gmax), jnp.zeros((120, T), F32)], axis=0).T
    ones = jnp.ones((1, 128), F32)
    s8 = lax.broadcasted_iota(jnp.int32, (8, 128), 0)

    def state_copies(i, h):
        to = lax.rem(sp + steps[i], n_sp)
        return (remote(mem_out_b.at[i, h], mem_in_b.at[i, h], st_s.at[i, h, 0], st_r.at[i, h, 0], to_sp=to),
                remote(sm_out.at[i, h], sm_in.at[i, h], st_s.at[i, h, 1], st_r.at[i, h, 1], to_sp=to))

    def state_send(i, h, vec, mem):
        n, d, m = vec
        mem_out_b[i, h] = mem.astype(BF16)
        sm_out[i, h] = jnp.where(s8 == 0, n, jnp.where(s8 == 1, d, m))
        for cp in state_copies(i, h):
            cp.start()
            sends.append(cp)

    zero = jnp.zeros((1, 128), F32)
    incl, excl = [None] * heads, [(zero, zero, jnp.full((1, 128), NEG, F32))] * heads
    for h in range(heads):
        keyed = PJ[:, h * KEY_DIM:(h + 1) * KEY_DIM].astype(F32) * COL[:, h:h + 1]
        norm = jnp.sum(keyed, axis=0, keepdims=True)
        mem = mm(keyed.T.astype(BF16), PJ[:, o_v + h * VALUE_DIM:o_v + (h + 1) * VALUE_DIM])
        A_mem[h] = mem
        incl[h] = (norm, decay[h:h + 1] * ones, (decay[h:h + 1] + gmax[h:h + 1]) * ones)
        state_send(0, h, incl[h], mem)
    E_mem[...] = jnp.zeros_like(E_mem)

    def join(valid, early, early_mem, late, late_mem):
        n_e, d_e, m_e = early
        n_l, d_l, m_l = late
        d_e = jnp.where(valid, d_e, 0.0)
        m_e = jnp.where(valid, m_e, NEG)
        top = jnp.maximum(m_e + d_l, m_l)
        s_e = jnp.where(valid, jnp.exp(m_e + d_l - top), 0.0)
        s_l = jnp.exp(m_l - top)
        return ((s_e * n_e + s_l * n_l, d_e + d_l, top),
                s_e[:, 0:1] * early_mem + s_l[:, 0:1] * late_mem)

    def state_step(i, h):
        for cp in state_copies(i, h):
            cp.wait_recv()
        valid = sp >= steps[i]
        got = sm_in[i, h]
        early = (got[0:1], got[1:2], got[2:3])
        early_mem = mem_in_b[i, h].astype(F32)
        if i + 1 < len(steps):
            incl[h], mem = join(valid, early, early_mem, incl[h], A_mem[h])
            A_mem[h] = mem
            state_send(i + 1, h, incl[h], mem)
        excl[h], mem = join(valid, early, early_mem, excl[h], E_mem[h])
        E_mem[h] = mem

    def work_running_max():
        run = gap
        for d in scan_steps(T):
            run = jnp.maximum(run, jnp.where(lane >= d, pltpu.roll(run, d, 1), run))
        COL[...] = jnp.concatenate([run, jnp.zeros((120, T), F32)], axis=0).T

    rb = 256 if T % 256 == 0 else R

    def work_project(first, last):
        for b in others:
            project(b, first, last)

    halo = remote(halo_out, halo_in, hl_s.at[0], hl_s.at[1], to_sp=lax.rem(sp + 1, n_sp))

    def work_product():
        for r0 in range(0, T, rb):
            left = PJ[r0:r0 + rb, o_c + channels:o_c + 2 * channels].astype(F32)
            right = PJ[r0:r0 + rb, o_c + 2 * channels:o_c + 3 * channels].astype(F32)
            prod = (left * right).astype(BF16)
            PROD[8 + r0:8 + r0 + rb, :] = prod.astype(F32)
            if r0 + rb == T:
                halo_out[...] = prod[rb - 16:rb]
        halo.start()
        sends.append(halo)

    q_scale = KEY_DIM ** -0.5

    def attend(h, r0):
        e = r0 + rb
        q = PJ[r0:e, o_q + h * KEY_DIM:o_q + (h + 1) * KEY_DIM]
        k = PJ[0:e, h * KEY_DIM:(h + 1) * KEY_DIM]
        v = PJ[0:e, o_v + h * VALUE_DIM:o_v + (h + 1) * VALUE_DIM]
        s = mm_t(q, k) * q_scale
        ti = lax.broadcasted_iota(jnp.int32, (rb, e), 0) + r0
        si = lax.broadcasted_iota(jnp.int32, (rb, e), 1)
        w = jnp.where(ti >= si, gap[h:h + 1, 0:e] - COL[r0:e, h:h + 1], NEG)
        mix = s * jnp.exp(w)
        DEN[h, r0:e, :] = jnp.broadcast_to(jnp.sum(mix, axis=1, keepdims=True), (rb, 128))
        NUM[r0:e, h * VALUE_DIM:(h + 1) * VALUE_DIM] = mm(mix.astype(BF16), v)

    work = [functools.partial(attend, h, r0) for h in range(heads) for r0 in range(0, T, rb)]

    def conv_finish():
        halo.wait_recv()
        before = halo_in[...].astype(F32)[8:16]
        PROD[0:8, :] = jnp.where(sp > 0, before, 0.0)
        tap = taps[:, pl.ds(pl.multiple_of(tp * channels, 128), channels)]
        for r0 in range(0, T, rb):
            f = tap[0:1] * PROD[6 + r0:6 + r0 + rb, :]
            f = f + tap[1:2] * PROD[7 + r0:7 + r0 + rb, :]
            f = f + tap[2:3] * PROD[8 + r0:8 + r0 + rb, :]
            gate = PJ[r0:r0 + rb, o_c:o_c + channels].astype(F32)
            HC[r0:r0 + rb, vw:] = (gate * f).astype(BF16)

    c1 = o_c + channels
    slots = [
        [functools.partial(work_project, o_q, c1), work_running_max],
        [functools.partial(work_project, c1, total)],
        [work_product, work.pop(0)],
    ]
    events = [(i, h) for i in range(len(steps)) for h in range(heads)]
    rest = work + [conv_finish]
    for n, event in enumerate(events[:-heads]):
        for w_ in (slots.pop(0) if slots else [rest.pop(0)] if rest else []):
            w_()
        state_step(*event)
    for group in slots:
        for w_ in group:
            w_()
    for w_ in rest:
        w_()

    sq = [jnp.zeros((rb, 1), F32) for _ in range(T // rb)]
    for h in range(heads):
        state_step(len(steps) - 1, h)
        n_e, d_e, m_e = excl[h]
        cmax = jnp.maximum(m_e, d_e)
        s_p, s_f = jnp.exp(m_e - cmax), jnp.exp(d_e - cmax)
        c_mem = s_p[:, 0:1] * E_mem[h] + s_f[:, 0:1] * first_mem[h]
        c_norm = s_p * n_e + s_f * first_norm[h:h + 1, :]
        hi = c_mem.astype(BF16)
        lo = (c_mem - hi.astype(F32)).astype(BF16)
        for b, r0 in enumerate(range(0, T, rb)):
            e = r0 + rb
            q = PJ[r0:e, o_q + h * KEY_DIM:o_q + (h + 1) * KEY_DIM]
            fm = mm(q, hi) + mm(q, lo)
            fn = jnp.sum(q.astype(F32) * c_norm, axis=1, keepdims=True)
            m0 = COL[r0:e, h:h + 1]
            m = jnp.maximum(m0, cmax[:, 0:1])
            k0 = jnp.exp(m0 - m)
            k1 = jnp.exp(cmax[:, 0:1] - m) * q_scale
            den = k0 * DEN[h, r0:e, 0:1] + k1 * fn
            inv = 1.0 / jnp.maximum(jnp.abs(den), 1.0)
            cols = slice(h * VALUE_DIM, (h + 1) * VALUE_DIM)
            mo = (k0 * NUM[r0:e, cols] + k1 * fm) * inv
            NUM[r0:e, cols] = mo
            sq[b] = sq[b] + jnp.sum(mo * mo, axis=1, keepdims=True)
    sq_col = jnp.concatenate([jnp.broadcast_to(s, (rb, 128)) for s in sq], axis=0)
    mine = sq_col.T[0:8]
    sq_out[...] = mine
    for k in range(1, n_tp):
        cp = remote(sq_out, sq_in.at[k - 1], sq_s.at[k - 1], sq_r.at[k - 1], to_tp=lax.rem(tp + k, n_tp))
        cp.start()
        sends.append(cp)
    tot = mine
    for k in range(1, n_tp):
        remote(sq_out, sq_in.at[k - 1], sq_s.at[k - 1], sq_r.at[k - 1], to_tp=partner).wait_recv()
        tot = tot + sq_in[k - 1]
    r_scale = lax.rsqrt(tot / float(width) + EPS)
    COL[...] = jnp.concatenate([r_scale] * 16, axis=0).T
    for r0 in range(0, T, rb):
        HC[r0:r0 + rb, 0:vw] = (NUM[r0:r0 + rb, :] * COL[r0:r0 + rb, 0:1]).astype(BF16)

    for c in w_copies[6:]:
        c.wait()
    cw = D // RS_CHUNKS

    def out_block(chip_row, idx, j):
        cols = pl.ds(pl.multiple_of(j * cw, 128), cw)
        rr = rows_of(chip_row, 2)
        PS[rr, cols] = mm(HC[rr, :], WO[:, cols]).astype(BF16)
        return remote(PS.at[rows_of(chip_row + 1 - core), cols], DR.at[idx, :, cols],
                      rd_s.at[idx, j], rd_r.at[idx, j], to_tp=partner)

    def pair_sum(chip_row, idx, j):
        cols = pl.ds(pl.multiple_of(j * cw, 128), cw)
        mine_rows = rows_of(chip_row + core)
        remote(PS.at[mine_rows, cols], DR.at[idx, :, cols], rd_s.at[idx, j], rd_r.at[idx, j],
               to_tp=partner).wait_recv()
        return cols, PS[mine_rows, cols].astype(F32) + DR[idx, :, cols].astype(F32)

    def y_copy(k, j):
        cols = pl.ds(pl.multiple_of(j * cw, 128), cw)
        return remote(YS.at[k - 1, :, cols], YR.at[k - 1, :, cols], ry_s.at[k - 1, j], ry_r.at[k - 1, j],
                      to_tp=lax.rem(y + k, n_y) * 2 + core)

    for k in range(1, n_y):
        def one(j, _, k=k):
            @pl.when(j < RS_CHUNKS)
            def _():
                out_block(others[k - 1], k, j).start()

            @pl.when(j > 0)
            def _():
                cols, s = pair_sum(others[k - 1], k, j - 1)
                YS[k - 1, :, cols] = s.astype(BF16)
                y_copy(k, j - 1).start()
            return 0

        lax.fori_loop(0, RS_CHUNKS + 1, one, 0)

    def local(j, _):
        out_block(2 * y, 0, j).start()
        return 0

    lax.fori_loop(0, RS_CHUNKS, local, 0)

    def finish(j, _):
        cols, s = pair_sum(2 * y, 0, j)
        for k in range(1, n_y):
            y_copy(k, j).wait_recv()
            s = s + YR[k - 1, :, cols].astype(F32)
        out[:, cols] = s.astype(BF16)
        return 0

    lax.fori_loop(0, RS_CHUNKS, finish, 0)

    for cp in sends:
        cp.wait_send()
    own.wait_send()

    def drain(j, _):
        for idx in range(n_y):
            cols = pl.ds(pl.multiple_of(j * cw, 128), cw)
            remote(PS.at[rows_of(2 * y + core), cols], DR.at[idx, :, cols], rd_s.at[idx, j],
                   rd_r.at[idx, j], to_tp=partner).wait_send()
        for k in range(1, n_y):
            y_copy(k, j).wait_send()
        return 0

    lax.fori_loop(0, RS_CHUNKS, drain, 0)


def per_device(
    n_sp, n_tp,
    tokens, in_gain, w_query, w_key, w_value, w_input_gate, w_forget_gate, forget_bias,
    forget_extra, w_conv_gate, w_conv_left, w_conv_right, conv_taps, first_memory, first_norm,
    w_out_memory, w_out_conv,
):
    heads = w_query.shape[1] // KEY_DIM
    channels = w_conv_gate.shape[1]
    R, D = tokens.shape
    T = R * n_tp
    n_y = n_tp // 2
    qk, vw = heads * KEY_DIM, heads * VALUE_DIM
    total = 2 * qk + vw + 128 + 3 * channels
    n_heads = w_input_gate.shape[1]
    n_st = len(scan_steps(n_sp))
    vmem = pl.BlockSpec(memory_space=pltpu.VMEM)
    hbm = pl.BlockSpec(memory_space=pl.ANY)
    V, dma = pltpu.VMEM, pltpu.SemaphoreType.DMA
    ny1 = n_y - 1
    return pl.pallas_call(
        functools.partial(kernel, n_sp, n_tp, heads, channels, n_heads * VALUE_DIM),
        out_shape=jax.ShapeDtypeStruct((R, D), BF16),
        in_specs=[vmem, vmem] + [hbm] * 6 + [vmem] * 2
        + [pl.BlockSpec(memory_space=pltpu.SMEM)] + [vmem] * 4 + [hbm] * 2,
        out_specs=vmem,
        scratch_shapes=[
            V((D, total), BF16), V((vw + channels, D), BF16), V((T, D), BF16), V((T, total), BF16),
            V((T, 128), F32), V((T, 128), F32), V((T, vw), F32), V((heads, T, 128), F32),
            V((T, vw + channels), BF16), V((8 + T, channels), F32),
            V((16, channels), BF16), V((16, channels), BF16),
            V((heads, KEY_DIM, VALUE_DIM), F32), V((heads, KEY_DIM, VALUE_DIM), F32),
            V((n_st, heads, 8, 128), F32), V((n_st, heads, 8, 128), F32),
            V((n_st, heads, KEY_DIM, VALUE_DIM), BF16), V((n_st, heads, KEY_DIM, VALUE_DIM), BF16),
            V((8, T), F32), V((n_tp - 1, 8, T), F32),
            V((T, D), BF16), V((n_y, R, D), BF16), V((ny1, R, D), BF16), V((ny1, R, D), BF16),
            dma((8,)), dma((2,)), dma((ny1, AG_CHUNKS)), dma((ny1, AG_CHUNKS)),
            dma((ny1, AG_CHUNKS)), dma((ny1, AG_CHUNKS)), dma((n_st, heads, 2)), dma((n_st, heads, 2)), dma((2,)),
            dma((n_tp - 1,)), dma((n_tp - 1,)),
            dma((n_y, RS_CHUNKS)), dma((n_y, RS_CHUNKS)), dma((ny1, RS_CHUNKS)), dma((ny1, RS_CHUNKS)),
        ],
        compiler_params=pltpu.CompilerParams(
            collective_id=0, has_side_effects=True, vmem_limit_bytes=60 * 1024 * 1024),
        name="layer",
    )(
        tokens, in_gain.reshape(1, D), w_key, w_value, w_query, w_conv_gate, w_conv_left,
        w_conv_right, w_input_gate.T, w_forget_gate.T, forget_bias, forget_extra.T, conv_taps, first_memory, first_norm,
        w_out_memory, w_out_conv,
    )


def solution(mesh):
    in_specs = (
        P(("sp", "tp"), None), P(), P(None, "tp"), P(None, "tp"), P(None, "tp"), P(), P(), P(),
        P("sp", "tp"), P(None, "tp"), P(None, "tp"), P(None, "tp"), P(), P("tp", None, None),
        P("tp", None), P("tp", None), P("tp", None),
    )
    return jax.shard_map(
        functools.partial(per_device, mesh.shape["sp"], mesh.shape["tp"]),
        mesh=mesh, in_specs=in_specs, out_specs=P(("sp", "tp"), None), check_vma=False,
    )
```

profile of v0, /device:TPU:0, one launch (start us, length us, event | category | flops | bytes accessed | tf_op | source)
XLA Modules:
  0.0 74.8 jit_solution(4045039312275081459)
XLA Ops:
  0.0 72.7 %layer.1 = bf16[192,2048]{1,0:T(8,128)(2,1)} custom-call(bf16[192,2048]{1,0:T(8,128)(2,1)} %tokens.1, f32[1,2048]{1,0:T(1,128)} %bitcast.6, bf16[2048,256]{1,0:T(8,128)(2,1)} %wk.1, bf16[2048,512]{1,0:T(8,128)(2,1)} %wv.1, bf16[2048,256]{1,0:T(8,128)(2,1)} %wq.1, bf16[2048,512]{1,0:T(8,128)(2,1)} %wcg.1, bf16[2048,512]{1,0:T(8,128)(2,1)} %wcl.1, ...), custom_call_target="tpu_custom_call" | custom-call | tf_op jit(solution)/shard_map/layer/pallas_call | solution.py:430
  72.7 2.1 %copy.19 = bf16[192,2048]{1,0:T(8,128)(2,1)} copy(bf16[192,2048]{1,0:T(8,128)(2,1)} %layer.1) | data formatting | bytes 1572864
where the time goes:
time: 74.9 us; the launch traced here: 74.8 us
  Pallas kernels  72.7 us (97%)
  local copies, waits for them, and re-layouts  2.09 us (3%)
    pallas_call x1, Pallas kernels, per_device(): pl.pallas_call(functools.partial(kernel, n_sp, n_tp, heads, channels, n_h...  72.7 us
    unnamed x1, local copies, waits for them, and re-layouts  2.09 us

commit v1 on v0

v1 whole, which is shorter than its diff:
```python
import functools
import math

import jax
import jax.numpy as jnp
from jax import lax
from jax.experimental import pallas as pl
from jax.experimental.pallas import tpu as pltpu
from jax.sharding import PartitionSpec as P

KEY_DIM = 128
VALUE_DIM = 256
TAPS = 3
EPS = 1e-06
NEG = -1e30
MESH = pl.DeviceIdType.MESH
F32 = jnp.float32
BF16 = jnp.bfloat16
RS_CHUNKS = 8
PARTS = 4
MAX_SLOTS = 3


def mm(a, b):
    return lax.dot_general(a, b, (((1,), (0,)), ((), ())), preferred_element_type=F32)


def mm_t(a, b):
    return lax.dot_general(a, b, (((1,), (1,)), ((), ())), preferred_element_type=F32)


def scan_steps(n):
    steps, d = [], 1
    while d < n:
        steps.append(d)
        d *= 2
    return steps


def group_size(n_sp):
    b = 1
    while (2 * b) ** 2 <= n_sp and n_sp % (2 * b) == 0:
        b *= 2
    return b


def gather_pieces(rows):
    third = rows // 3
    return [(0, third), (third, third), (2 * third, third - 16), (rows - 16, 16)]


def kernel(
    n_sp, n_tp, heads, channels, width,
    tokens_h, gain_h, wk, wv, wq, wcg, wcl, wcr, wig_h, wfg_h, bias_h, extra_h, taps_h, first_mem_h, first_norm_h,
    wom, woc, out,
    TK, gain, wig, wfg, bias, extra, taps, first_mem, first_norm,
    W, WO, XG, PJ, G, RM, NUM, DEN, MO, CB, PROD, halo_out, halo_in,
    ST, SM, CO, CI, CSO, CSI, sq_out, sq_in, RC,
    PSC, PSM, DRC, DRM, YS, YR,
    i_sem, w_sem, ag_d, ag_ys, ag_yr, ag_fs, ag_fr, xs_s, xs_r, ch_s, ch_r, hl_s, sq_s, sq_r,
    cd_s, cd_r, rd_s, rd_r, ry_s, ry_r, ent,
):
    sp = lax.axis_index("sp")
    tp = lax.axis_index("tp")
    core = lax.rem(tp, 2)
    y = tp // 2
    n_y = n_tp // 2
    partner = tp + 1 - 2 * core
    R, D = TK.shape
    T = R * n_tp
    B = group_size(n_sp)
    A = n_sp // B
    zg, x_in = sp // B, lax.rem(sp, B)
    qk, vw = heads * KEY_DIM, heads * VALUE_DIM
    o_v, o_g = qk, qk + vw
    o_q = o_g + 128
    o_c = o_q + qk
    total = o_c + 3 * channels
    n_heads = wig.shape[0]

    def remote(src, dst, ss, rs, to_tp=None, to_sp=None):
        return pltpu.make_async_remote_copy(
            src_ref=src, dst_ref=dst, send_sem=ss, recv_sem=rs,
            device_id=(sp if to_sp is None else to_sp, tp if to_tp is None else to_tp),
            device_id_type=MESH,
        )

    barrier = pltpu.get_barrier_semaphore()
    for k in range(1, n_tp):
        pl.semaphore_signal(barrier, inc=1, device_id=(sp, lax.rem(tp + k, n_tp)), device_id_type=MESH)

    def later(fn):
        for k in range(1, B):
            pl.when(x_in + k < B)(functools.partial(fn, k))
        pl.when(zg < A - 1)(functools.partial(fn, B))
        if B > 1:
            pl.when((x_in == B - 1) & (zg < A - 1))(functools.partial(fn, 1))

    def earlier(fn):
        for k in range(1, B):
            pl.when(x_in >= k)(functools.partial(fn, k))
        pl.when(zg > 0)(functools.partial(fn, B))
        if B > 1:
            pl.when((x_in == 0) & (zg > 0))(functools.partial(fn, 1))

    extra_link = 1 if B > 1 else 0
    n_earlier = x_in + jnp.where(zg > 0, 1, 0) + extra_link * jnp.where((x_in == 0) & (zg > 0), 1, 0)
    n_later = (B - 1 - x_in + jnp.where(zg < A - 1, 1, 0)
               + extra_link * jnp.where((x_in == B - 1) & (zg < A - 1), 1, 0))
    later(lambda k: pl.semaphore_signal(barrier, inc=1, device_id=(sp + k, tp), device_id_type=MESH))

    inputs = [(tokens_h, TK), (gain_h, gain), (wig_h, wig), (wfg_h, wfg), (bias_h, bias), (extra_h, extra),
              (taps_h, taps), (first_mem_h, first_mem), (first_norm_h, first_norm)]
    in_copies = [pltpu.make_async_copy(s, d, i_sem.at[i]) for i, (s, d) in enumerate(inputs)]
    for c in in_copies[:4]:
        c.start()
    srcs = [(wk, 0, qk), (wv, o_v, vw), (wq, o_q, qk), (wcg, o_c, channels),
            (wcl, o_c + channels, channels), (wcr, o_c + 2 * channels, channels)]
    w_copies = [
        pltpu.make_async_copy(s, W.at[:, pl.ds(o, n)], w_sem.at[i])
        for i, (s, o, n) in enumerate(srcs)
    ]
    w_copies.append(pltpu.make_async_copy(woc, WO.at[pl.ds(vw, channels), :], w_sem.at[6]))
    w_copies.append(pltpu.make_async_copy(wom, WO.at[pl.ds(0, vw), :], w_sem.at[7]))
    for c in w_copies:
        c.start()
    for c in in_copies[4:]:
        c.start()

    def rows_of(block, first=0, n=None):
        n = R if n is None else n
        return pl.ds(pl.multiple_of(block * R + first, 16), n)

    def chip_rows(chip):
        return pl.ds(pl.multiple_of(chip * 2 * R, 16), 2 * R)

    in_copies[0].wait()
    in_copies[1].wait()
    x = TK[...].astype(F32)
    scale = lax.rsqrt(jnp.mean(x * x, axis=1, keepdims=True) + EPS)
    XG[rows_of(tp), :] = (x * scale * gain[...]).astype(BF16)
    pl.semaphore_wait(barrier, n_tp - 1 + n_earlier)
    earlier(lambda k: pl.semaphore_signal(ent, inc=1, device_id=(sp - k, tp), device_id_type=MESH))

    pieces = gather_pieces(R)
    third = R // 3
    sends = []

    def far_rows(chip, c, src_core):
        first, n = pieces[c]
        part = min(c, 2)
        at = chip * 2 * R + 2 * third * part + src_core * third + (first - part * third)
        return pl.ds(pl.multiple_of(at, 16), n)

    def y_piece(k, c, chip, to):
        src = XG.at[rows_of(tp, pieces[c][0], pieces[c][1]), :]
        return remote(src, XG.at[far_rows(chip, c, core), :], ag_ys.at[k - 1, c], ag_yr.at[k - 1, c], to_tp=to)

    for c in range(len(pieces)):
        for k in range(1, n_y):
            cp = y_piece(k, c, y, lax.rem(y + k, n_y) * 2 + core)
            cp.start()
            sends.append(cp)
    own = remote(XG.at[rows_of(tp), :], XG.at[rows_of(tp), :], ag_d.at[0], ag_d.at[1], to_tp=partner)
    own.start()

    def source(k):
        return lax.rem(y + n_y - k, n_y)

    def forward(c):
        for k in range(1, n_y):
            chip = source(k)
            y_piece(k, c, chip, partner).wait_recv()
            r = far_rows(chip, c, core)
            cp = remote(XG.at[r, :], XG.at[r, :], ag_fs.at[k - 1, c], ag_fr.at[k - 1, c], to_tp=partner)
            cp.start()
            sends.append(cp)

    def forwarded(c):
        for k in range(1, n_y):
            r = far_rows(source(k), c, 1 - core)
            remote(XG.at[r, :], XG.at[r, :], ag_fs.at[k - 1, c], ag_fr.at[k - 1, c], to_tp=partner).wait_recv()

    kv_cols = [(0, o_g)]
    rest_cols = [(o_q, qk)] + [(o_c + i * channels, channels) for i in range(3)]

    def project_local(cols):
        rr = chip_rows(y)
        for first, n in cols:
            PJ[rr, first:first + n] = mm(XG[rr, :], W[:, first:first + n]).astype(BF16)

    def local_gates():
        rr = chip_rows(y)
        G[rr, :] = mm(XG[rr, :], W[:, o_g:o_g + 128])

    def far_parts(part, chip):
        rr = pl.ds(pl.multiple_of(chip * 2 * R + 2 * third * part, 16), 2 * third)
        return rr, [rows_of(2 * chip + i, part * third, third) for i in range(2)]

    def project_far(part, cols):
        for k in range(1, n_y):
            rr, to = far_parts(part, source(k))
            for first, n in cols:
                res = mm(XG[rr, :], W[:, first:first + n]).astype(BF16)
                for i in range(2):
                    PJ[to[i], first:first + n] = res[i * third:(i + 1) * third]

    def far_gates(part):
        for k in range(1, n_y):
            rr, to = far_parts(part, source(k))
            res = mm(XG[rr, :], W[:, o_g:o_g + 128])
            for i in range(2):
                G[to[i], :] = res[i * third:(i + 1) * third]

    in_copies[2].wait()
    in_copies[3].wait()
    W[:, o_g:o_g + 128] = jnp.concatenate(
        [wig[...].astype(F32), wfg[...].astype(F32), jnp.zeros((128 - 2 * n_heads, D), F32)],
        axis=0).T.astype(BF16)
    for c in in_copies[4:]:
        c.wait()
    for c in w_copies[:2]:
        c.wait()
    own.wait_recv()
    project_local(kv_cols)
    local_gates()
    for c in w_copies[2:6]:
        c.wait()
    project_local(rest_cols)
    for part in range(2):
        forward(part)
        forwarded(part)
        project_far(part, kv_cols)
        far_gates(part)
        project_far(part, rest_cols)
    forward(2)
    forward(3)
    forwarded(2)
    forwarded(3)
    far_gates(2)
    project_far(2, kv_cols)

    gt = G[...].T
    in_all, forget_all = gt[0:n_heads], gt[n_heads:2 * n_heads]
    sub = lax.broadcasted_iota(jnp.int32, (n_heads, T), 0)
    sub8 = lax.broadcasted_iota(jnp.int32, (8, T), 0)
    lane = lax.broadcasted_iota(jnp.int32, (8, T), 1)
    in_pre = jnp.zeros((8, T), F32)
    log_f = jnp.zeros((8, T), F32)
    for h in range(heads):
        head = tp * heads + h
        row_i = jnp.sum(jnp.where(sub == head, in_all, 0.0), axis=0, keepdims=True)
        row_f = jnp.sum(jnp.where(sub == head, forget_all, 0.0), axis=0, keepdims=True) + bias[head]
        row_f = jnp.minimum(row_f, 0.0) - jnp.log1p(jnp.exp(-jnp.abs(row_f))) + extra[h:h + 1, :]
        in_pre = jnp.where(sub8 == h, row_i, in_pre)
        log_f = jnp.where(sub8 == h, row_f, log_f)
    cum = log_f
    for d in scan_steps(T):
        cum = cum + jnp.where(lane >= d, pltpu.roll(cum, d, 1), 0.0)
    gap = in_pre - cum
    decay = cum[:, T - 1:T]
    gmax = jnp.max(gap, axis=1, keepdims=True)
    w_all = jnp.exp(gap - gmax)
    w_hi = w_all.astype(BF16)
    w_lo = (w_all - w_hi.astype(F32)).astype(BF16)
    w_two = jnp.concatenate([w_hi, w_lo], axis=0)
    ones = jnp.ones((1, 128), F32)
    s8 = lax.broadcasted_iota(jnp.int32, (8, 128), 0)
    pr = KEY_DIM // PARTS

    def group_copies(k, h, p):
        to = sp - x_in + lax.rem(x_in + k, B)
        if p == 0:
            ref = SM.at[x_in, h]
        else:
            ref = ST.at[x_in, h, pl.ds((p - 1) * pr, pr), :]
        return remote(ref, ref, xs_s.at[k - 1, h, p], xs_r.at[k - 1, h, p], to_sp=to)

    def group_sends(fn):
        for k in range(1, B):
            pl.when((zg < A - 1) | (x_in + k < B))(functools.partial(fn, k))

    pl.when(sp < n_sp - 1)(lambda: pl.semaphore_wait(ent, n_later))
    for h in range(heads):
        k_t = PJ[:, h * KEY_DIM:(h + 1) * KEY_DIM].T
        keyed = (k_t.astype(F32) * w_all[h:h + 1, :]).astype(BF16)
        n2 = mm(w_two, PJ[:, h * KEY_DIM:(h + 1) * KEY_DIM])
        norm = n2[h:h + 1] + n2[8 + h:9 + h]
        d_row = decay[h:h + 1] * ones
        m_row = (decay[h:h + 1] + gmax[h:h + 1]) * ones
        SM[x_in, h] = jnp.where(s8 == 0, norm, jnp.where(s8 == 1, d_row, m_row))
        ST[x_in, h] = mm(keyed, PJ[:, o_v + h * VALUE_DIM:o_v + (h + 1) * VALUE_DIM]).astype(BF16)

        def go(k, h=h):
            for p in range(PARTS + 1):
                group_copies(k, h, p).start()

        group_sends(go)

    def weights(h, limit):
        valid = [j < limit for j in range(B)]
        ds = [jnp.where(valid[j], SM[j, h, 1:2], 0.0) for j in range(B)]
        ms = [jnp.where(valid[j], SM[j, h, 2:3], NEG) for j in range(B)]
        ns = [jnp.where(valid[j], SM[j, h, 0:1], 0.0) for j in range(B)]
        c_m = jnp.where(zg > 0, CSI[h, 2:3], 0.0)
        c_n = jnp.where(zg > 0, CSI[h, 0:1], first_norm[h:h + 1, :])
        after = [jnp.zeros((1, 128), F32)] * B
        for j in range(B - 2, -1, -1):
            after[j] = after[j + 1] + ds[j + 1]
        c_m = c_m + after[0] + ds[0]
        top = c_m
        for j in range(B):
            top = jnp.maximum(top, ms[j] + after[j])
        c_c = jnp.exp(c_m - top)
        c_j = [jnp.where(valid[j], jnp.exp(ms[j] + after[j] - top), 0.0) for j in range(B)]
        norm = c_c * c_n
        for j in range(B):
            norm = norm + c_j[j] * ns[j]
        return c_c, c_j, valid, norm, top

    def joined(h, wts, first, n):
        c_c, c_j, valid = wts[:3]
        two = lambda v: jnp.concatenate([v] * (VALUE_DIM // 128), axis=1)
        r = slice(first, first + n)
        mem = two(c_c) * jnp.where(zg > 0, CI[h, r].astype(F32), first_mem[h, r])
        for j in range(B):
            mem = mem + two(c_j[j]) * jnp.where(valid[j], ST[j, h, r].astype(F32), 0.0)
        return mem

    def chain_copy(h, p):
        if p == 0:
            s, d = CSO.at[h], CSI.at[h]
        else:
            rr = pl.ds((p - 1) * pr, pr)
            s, d = CO.at[h, rr, :], CI.at[h, rr, :]
        return remote(s, d, ch_s.at[h, p], ch_r.at[h, p], to_sp=sp + B)

    def chain_wait(h, p):
        if p == 0:
            d = CSI.at[h]
        else:
            d = CI.at[h, pl.ds((p - 1) * pr, pr), :]
        remote(d, d, ch_s.at[h, p], ch_r.at[h, p], to_tp=partner).wait_recv()

    def group_wait(k, h, p):
        j = lax.rem(x_in + B - k, B)
        d = SM.at[j, h] if p == 0 else ST.at[j, h, pl.ds((p - 1) * pr, pr), :]
        remote(d, d, xs_s.at[k - 1, h, p], xs_r.at[k - 1, h, p], to_tp=partner).wait_recv()

    def relay(chained):
        for h in range(heads):
            wts = None
            for p in range(PARTS + 1):
                for k in range(1, B):
                    group_wait(k, h, p)
                if chained:
                    chain_wait(h, p)
                if p == 0:
                    wts = weights(h, B)
                    CSO[h] = jnp.where(s8 == 0, wts[3], wts[4])
                else:
                    CO[h, (p - 1) * pr:p * pr] = joined(h, wts, (p - 1) * pr, pr).astype(BF16)
                chain_copy(h, p).start()

    def slot(s):
        last = min(MAX_SLOTS, A - 1)
        if s < last:
            pl.when(zg == s)(functools.partial(relay, s > 0))
        if s == last:
            if A - 1 > last:
                pl.when((zg >= last) & (zg < A - 1))(functools.partial(relay, True))

            @pl.when(zg == A - 1)
            def _():
                for h in range(heads):
                    for p in range(PARTS + 1):
                        for k in range(1, B):
                            pl.when(k <= x_in)(functools.partial(group_wait, k, h, p))
                        if A > 1:
                            chain_wait(h, p)

    rb = 256 if T % 256 == 0 else R
    q_scale = KEY_DIM ** -0.5
    shifted = gap + math.log(q_scale)

    def work_running_max():
        run = gap
        for d in scan_steps(T):
            run = jnp.maximum(run, jnp.where(lane >= d, pltpu.roll(run, d, 1), run))
        for h in range(heads):
            RM[h] = jnp.broadcast_to(run[h:h + 1], (128, T)).T

    def halo_copy(to):
        return remote(halo_out, halo_in, hl_s.at[0], hl_s.at[1], to_sp=to)

    def work_product():
        for r0 in range(0, T, rb):
            left = PJ[r0:r0 + rb, o_c + channels:o_c + 2 * channels].astype(F32)
            right = PJ[r0:r0 + rb, o_c + 2 * channels:o_c + 3 * channels].astype(F32)
            prod = (left * right).astype(BF16)
            PROD[8 + r0:8 + r0 + rb, :] = prod.astype(F32)
            if r0 + rb == T:
                halo_out[...] = prod[rb - 16:rb]
        pl.when(sp < n_sp - 1)(lambda: halo_copy(sp + 1).start())

    def attend(h, r0):
        e = r0 + rb
        q = PJ[r0:e, o_q + h * KEY_DIM:o_q + (h + 1) * KEY_DIM]
        k = PJ[0:e, h * KEY_DIM:(h + 1) * KEY_DIM]
        v = PJ[0:e, o_v + h * VALUE_DIM:o_v + (h + 1) * VALUE_DIM]
        s = mm_t(q, k)
        ti = lax.broadcasted_iota(jnp.int32, (rb, rb), 0)
        si = lax.broadcasted_iota(jnp.int32, (rb, rb), 1)
        rm = RM[h, r0:e, :]
        w = shifted[h:h + 1, 0:e] - jnp.concatenate([rm] * (e // 128), axis=1)
        diag = jnp.where(ti >= si, w[:, r0:e], NEG)
        w = jnp.concatenate([w[:, 0:r0], diag], axis=1) if r0 else diag
        mix = s * jnp.exp(w)
        DEN[h, r0:e, :] = jnp.broadcast_to(jnp.sum(mix, axis=1, keepdims=True), (rb, 128))
        NUM[r0:e, h * VALUE_DIM:(h + 1) * VALUE_DIM] = mm(mix.astype(BF16), v)

    def conv_finish():
        @pl.when(sp > 0)
        def _():
            halo_copy(sp).wait_recv()
            PROD[0:8, :] = halo_in[...].astype(F32)[8:16]

        @pl.when(sp == 0)
        def _():
            PROD[0:8, :] = jnp.zeros((8, channels), F32)

        tap = taps[:, pl.ds(pl.multiple_of(tp * channels, 128), channels)]
        for r0 in range(0, T, rb):
            f = tap[0:1] * PROD[6 + r0:6 + r0 + rb, :]
            f = f + tap[1:2] * PROD[7 + r0:7 + r0 + rb, :]
            f = f + tap[2:3] * PROD[8 + r0:8 + r0 + rb, :]
            gate = PJ[r0:r0 + rb, o_c:o_c + channels].astype(F32)
            CB[r0:r0 + rb, :] = (gate * f).astype(BF16)

    cw = D // RS_CHUNKS
    chips = [y] + [lax.rem(y + k, n_y) for k in range(1, n_y)]
    order = list(range(1, n_y)) + [0]

    def conv_copy(idx):
        return remote(PSC.at[rows_of(2 * chips[idx] + 1 - core), :], DRC.at[idx], cd_s.at[idx], cd_r.at[idx],
                      to_tp=partner)

    def conv_out():
        w_copies[6].wait()
        for idx in order:
            rr = chip_rows(chips[idx])
            for j in range(RS_CHUNKS):
                cols = slice(j * cw, (j + 1) * cw)
                PSC[rr, cols] = mm(CB[rr, :], WO[vw:, cols]).astype(BF16)
            conv_copy(idx).start()

    work_running_max()
    project_far(2, rest_cols)
    slot(0)
    work_product()
    for r0 in range(0, T, rb):
        attend(0, r0)
    slot(1)
    for h in range(1, heads):
        for r0 in range(0, T, rb):
            attend(h, r0)
    conv_finish()
    slot(2)
    conv_out()
    slot(3)

    sq = [None] * (T // rb)
    for h in range(heads):
        wts = weights(h, x_in)
        c_mem = joined(h, wts, 0, KEY_DIM)
        c_norm, cmax = wts[3], wts[4]
        hi = c_mem.astype(BF16)
        lo = (c_mem - hi.astype(F32)).astype(BF16)
        two = jnp.concatenate([hi, lo], axis=0)
        n_col = jnp.broadcast_to(c_norm, (128, 128)).T
        n_hi = n_col.astype(BF16)
        n_lo = (n_col - n_hi.astype(F32)).astype(BF16)
        n_two = jnp.concatenate([n_hi, n_lo], axis=0)
        for b, r0 in enumerate(range(0, T, rb)):
            e = r0 + rb
            q = PJ[r0:e, o_q + h * KEY_DIM:o_q + (h + 1) * KEY_DIM]
            qq = jnp.concatenate([q, q], axis=1)
            fm = mm(qq, two)
            fn = mm(qq, n_two)
            m0 = RM[h, r0:e, :]
            m = jnp.maximum(m0, cmax)
            k0 = jnp.exp(m0 - m)
            k1 = jnp.exp(cmax - m) * q_scale
            den = k0 * DEN[h, r0:e, :] + k1 * fn
            inv = 1.0 / jnp.maximum(jnp.abs(den), 1.0)
            k0, k1 = k0 * inv, k1 * inv
            cols = slice(h * VALUE_DIM, (h + 1) * VALUE_DIM)
            mo = (jnp.concatenate([k0, k0], axis=1) * NUM[r0:e, cols]
                  + jnp.concatenate([k1, k1], axis=1) * fm)
            MO[r0:e, cols] = mo.astype(BF16)
            s2 = mo * mo
            s2 = s2[:, 0:128] + s2[:, 128:256]
            sq[b] = s2 if sq[b] is None else sq[b] + s2
    sq_out[...] = jnp.zeros_like(sq_out)
    for b in range(T // rb):
        row = jnp.sum(sq[b].T, axis=0, keepdims=True)
        for i in range(rb // 128):
            at = b * (rb // 128) + i
            sq_out[at:at + 1, :] = row[:, i * 128:(i + 1) * 128]
    for k in range(1, n_tp):
        cp = remote(sq_out, sq_in.at[k - 1], sq_s.at[k - 1], sq_r.at[k - 1], to_tp=lax.rem(tp + k, n_tp))
        cp.start()
        sends.append(cp)

    def cols_of(j):
        return pl.ds(j * cw, cw)

    def mem_copy(idx, j):
        return remote(PSM.at[rows_of(2 * chips[idx] + 1 - core), cols_of(j)], DRM.at[idx, :, cols_of(j)],
                      rd_s.at[idx, j], rd_r.at[idx, j], to_tp=partner)

    w_copies[7].wait()
    for idx in order:
        rr = chip_rows(chips[idx])
        for j in range(RS_CHUNKS):
            cols = slice(j * cw, (j + 1) * cw)
            PSM[rr, cols] = mm(MO[rr, :], WO[0:vw, cols]).astype(BF16)
            mem_copy(idx, j).start()
    for idx in order:
        conv_copy(idx).wait_recv()

    tot = sq_out[...]
    for k in range(1, n_tp):
        remote(sq_out, sq_in.at[k - 1], sq_s.at[k - 1], sq_r.at[k - 1], to_tp=partner).wait_recv()
        tot = tot + sq_in[k - 1]
    r_scale = lax.rsqrt(tot / float(width) + EPS)
    for b in range(T // 128):
        RC[b * 128:(b + 1) * 128, :] = jnp.broadcast_to(r_scale[b:b + 1], (128, 128)).T

    def chip_sum(idx, j):
        cols = slice(j * cw, (j + 1) * cw)
        mine = rows_of(2 * chips[idx] + core)
        mem_copy(idx, j).wait_recv()
        r = jnp.concatenate([RC[mine, :]] * (cw // 128), axis=1)
        s = (PSM[mine, cols].astype(F32) + DRM[idx, :, cols].astype(F32)) * r
        return s + (PSC[mine, cols].astype(F32) + DRC[idx, :, cols].astype(F32))

    def y_copy(k, j):
        return remote(YS.at[k - 1, :, cols_of(j)], YR.at[k - 1, :, cols_of(j)], ry_s.at[k - 1, j],
                      ry_r.at[k - 1, j], to_tp=lax.rem(y + k, n_y) * 2 + core)

    for j in range(RS_CHUNKS):
        for k in range(1, n_y):
            YS[k - 1, :, j * cw:(j + 1) * cw] = chip_sum(k, j).astype(BF16)
            y_copy(k, j).start()
    for j in range(RS_CHUNKS):
        s = chip_sum(0, j)
        for k in range(1, n_y):
            y_copy(k, j).wait_recv()
            s = s + YR[k - 1, :, j * cw:(j + 1) * cw].astype(F32)
        out[:, j * cw:(j + 1) * cw] = s.astype(BF16)

    for cp in sends:
        cp.wait_send()
    own.wait_send()
    for h in range(heads):
        for p in range(PARTS + 1):
            group_sends(lambda k, h=h, p=p: group_copies(k, h, p).wait_send())

            @pl.when(zg < A - 1)
            def _(h=h, p=p):
                chain_copy(h, p).wait_send()
    pl.when(sp < n_sp - 1)(lambda: halo_copy(sp + 1).wait_send())
    for idx in range(n_y):
        conv_copy(idx).wait_send()
        for j in range(RS_CHUNKS):
            mem_copy(idx, j).wait_send()
    for k in range(1, n_y):
        for j in range(RS_CHUNKS):
            y_copy(k, j).wait_send()


def per_device(
    n_sp, n_tp,
    tokens, in_gain, w_query, w_key, w_value, w_input_gate, w_forget_gate, forget_bias,
    forget_extra, w_conv_gate, w_conv_left, w_conv_right, conv_taps, first_memory, first_norm,
    w_out_memory, w_out_conv,
):
    heads = w_query.shape[1] // KEY_DIM
    channels = w_conv_gate.shape[1]
    R, D = tokens.shape
    T = R * n_tp
    n_y = n_tp // 2
    qk, vw = heads * KEY_DIM, heads * VALUE_DIM
    total = 2 * qk + vw + 128 + 3 * channels
    n_heads = w_input_gate.shape[1]
    B = group_size(n_sp)
    hbm = pl.BlockSpec(memory_space=pl.ANY)
    V, dma = pltpu.VMEM, pltpu.SemaphoreType.DMA
    ny1 = n_y - 1
    np_ = len(gather_pieces(R))
    sq_rows = -(-T // 1024) * 8
    return pl.pallas_call(
        functools.partial(kernel, n_sp, n_tp, heads, channels, n_heads * VALUE_DIM),
        out_shape=pltpu.VMEM((R, D), BF16),
        in_specs=[hbm] * 17,
        out_specs=pl.BlockSpec(memory_space=pltpu.VMEM),
        scratch_shapes=[
            V((R, D), BF16), V((1, D), F32), V((n_heads, D), BF16), V((n_heads, D), BF16),
            pltpu.SMEM((n_heads,), F32), V((heads, T), F32), V((TAPS, n_tp * channels), F32),
            V((heads, KEY_DIM, VALUE_DIM), F32), V((heads, KEY_DIM), F32),
            V((D, total), BF16), V((vw + channels, D), BF16), V((T, D), BF16), V((T, total), BF16),
            V((T, 128), F32), V((heads, T, 128), F32), V((T, vw), F32), V((heads, T, 128), F32),
            V((T, vw), BF16), V((T, channels), BF16), V((8 + T, channels), F32),
            V((16, channels), BF16), V((16, channels), BF16),
            V((B, heads, KEY_DIM, VALUE_DIM), BF16), V((B, heads, 8, 128), F32),
            V((heads, KEY_DIM, VALUE_DIM), BF16), V((heads, KEY_DIM, VALUE_DIM), BF16),
            V((heads, 8, 128), F32), V((heads, 8, 128), F32),
            V((sq_rows, 128), F32), V((n_tp - 1, sq_rows, 128), F32), V((T, 128), F32),
            V((T, D), BF16), V((T, D), BF16), V((n_y, R, D), BF16), V((n_y, R, D), BF16),
            V((ny1, R, D), BF16), V((ny1, R, D), BF16),
            dma((9,)), dma((8,)), dma((2,)), dma((ny1, np_)), dma((ny1, np_)),
            dma((ny1, np_)), dma((ny1, np_)),
            dma((B - 1, heads, PARTS + 1)), dma((B - 1, heads, PARTS + 1)),
            dma((heads, PARTS + 1)), dma((heads, PARTS + 1)), dma((2,)),
            dma((n_tp - 1,)), dma((n_tp - 1,)), dma((n_y,)), dma((n_y,)),
            dma((n_y, RS_CHUNKS)), dma((n_y, RS_CHUNKS)), dma((ny1, RS_CHUNKS)), dma((ny1, RS_CHUNKS)),
            pltpu.SemaphoreType.REGULAR,
        ],
        compiler_params=pltpu.CompilerParams(
            collective_id=0, has_side_effects=True, vmem_limit_bytes=60 * 1024 * 1024),
        name="layer",
    )(
        tokens, in_gain.reshape(1, D), w_key, w_value, w_query, w_conv_gate, w_conv_left,
        w_conv_right, w_input_gate.T, w_forget_gate.T, forget_bias, forget_extra.T, conv_taps, first_memory, first_norm,
        w_out_memory, w_out_conv,
    )


def solution(mesh):
    in_specs = (
        P(("sp", "tp"), None), P(), P(None, "tp"), P(None, "tp"), P(None, "tp"), P(), P(), P(),
        P("sp", "tp"), P(None, "tp"), P(None, "tp"), P(None, "tp"), P(), P("tp", None, None),
        P("tp", None), P("tp", None), P("tp", None),
    )
    return jax.shard_map(
        functools.partial(per_device, mesh.shape["sp"], mesh.shape["tp"]),
        mesh=mesh, in_specs=in_specs, out_specs=P(("sp", "tp"), None), check_vma=False,
    )
```

time: 74.9 us -> 62.1 us (0.83)
  Pallas kernels: 72.7 us -> 61.1 us
  local copies, waits for them, and re-layouts: 2.09 us -> 0.88 us
    pallas_call x1, Pallas kernels: 72.7 us -> 61.1 us  [per_device(): pl.pallas_call(functools.partial(kernel, n_sp, n_tp, heads, channels, n_h...]
    unnamed x1, local copies, waits for them, and re-layouts: 2.09 us -> 0.88 us
where the time goes in v1:
time: 62.1 us; the launch traced here: 62 us
  Pallas kernels  61.1 us (98%)
  local copies, waits for them, and re-layouts  0.88 us (1%)
    pallas_call x1, Pallas kernels, per_device(): pl.pallas_call(functools.partial(kernel, n_sp, n_tp, heads, channels, n_h...  61.1 us

profile of v1, /device:TPU:0, one launch (start us, length us, event | category | flops | bytes accessed | tf_op | source)
XLA Modules:
  0.0 62.0 jit_solution(11449285840164322768)
XLA Ops:
  0.0 61.1 %layer.1 = bf16[192,2048]{1,0:T(8,128)(2,1)S(1)} custom-call(bf16[192,2048]{1,0:T(8,128)(2,1)} %tokens_h.1, f32[1,2048]{1,0:T(1,128)} %bitcast.6, bf16[2048,256]{1,0:T(8,128)(2,1)} %wk.1, bf16[2048,512]{1,0:T(8,128)(2,1)} %wv.1, bf16[2048,256]{1,0:T(8,128)(2,1)} %wq.1, bf16[2048,512]{1,0:T(8,128)(2,1)} %wcg.1, bf16[2048,512]{1,0:T(8,128)(2,1)} %wcl.1, ...), custom_call_target="tpu_custom_call" | custom-call | tf_op jit(solution)/shard_map/layer/pallas_call | solution.py:603
  61.1 0.9 %copy.19 = bf16[192,2048]{1,0:T(8,128)(2,1)} copy(bf16[192,2048]{1,0:T(8,128)(2,1)S(1)} %layer.1) | data formatting | bytes 1572864

commit v2 on v1

--- a/solution.py
+++ b/solution.py
@@ -17,6 +17,7 @@
 F32 = jnp.float32
 BF16 = jnp.bfloat16
 RS_CHUNKS = 8
+EARLY = 1
 PARTS = 4
 MAX_SLOTS = 3
 
@@ -56,9 +57,8 @@
     TK, gain, wig, wfg, bias, extra, taps, first_mem, first_norm,
     W, WO, XG, PJ, G, RM, NUM, DEN, MO, CB, PROD, halo_out, halo_in,
     ST, SM, CO, CI, CSO, CSI, sq_out, sq_in, RC,
-    PSC, PSM, DRC, DRM, YS, YR,
-    i_sem, w_sem, ag_d, ag_ys, ag_yr, ag_fs, ag_fr, xs_s, xs_r, ch_s, ch_r, hl_s, sq_s, sq_r,
-    cd_s, cd_r, rd_s, rd_r, ry_s, ry_r, ent,
+    PSC, PSM, DRC, DRM, YS, YR, YC, YCR,
+    i_sem, s_sem, ag_d, ag_yr, ag_fr, xs_r, ch_r, hl_r, sq_r, cd_r, rd_r, ry_r, yc_r, ent,
 ):
     sp = lax.axis_index("sp")
     tp = lax.axis_index("tp")
@@ -109,22 +109,21 @@
                + extra_link * jnp.where((x_in == B - 1) & (zg < A - 1), 1, 0))
     later(lambda k: pl.semaphore_signal(barrier, inc=1, device_id=(sp + k, tp), device_id_type=MESH))
 
-    inputs = [(tokens_h, TK), (gain_h, gain), (wig_h, wig), (wfg_h, wfg), (bias_h, bias), (extra_h, extra),
-              (taps_h, taps), (first_mem_h, first_mem), (first_norm_h, first_norm)]
-    in_copies = [pltpu.make_async_copy(s, d, i_sem.at[i]) for i, (s, d) in enumerate(inputs)]
-    for c in in_copies[:4]:
-        c.start()
-    srcs = [(wk, 0, qk), (wv, o_v, vw), (wq, o_q, qk), (wcg, o_c, channels),
-            (wcl, o_c + channels, channels), (wcr, o_c + 2 * channels, channels)]
-    w_copies = [
-        pltpu.make_async_copy(s, W.at[:, pl.ds(o, n)], w_sem.at[i])
-        for i, (s, o, n) in enumerate(srcs)
-    ]
-    w_copies.append(pltpu.make_async_copy(woc, WO.at[pl.ds(vw, channels), :], w_sem.at[6]))
-    w_copies.append(pltpu.make_async_copy(wom, WO.at[pl.ds(0, vw), :], w_sem.at[7]))
-    for c in w_copies:
-        c.start()
-    for c in in_copies[4:]:
+    third = R // 3
+
+    def copies(sem, pairs):
+        return [pltpu.make_async_copy(a, b, i_sem.at[sem]) for a, b in pairs]
+
+    token_copies = [copies(i, [(tokens_h.at[r, :], TK.at[r, :])])[0]
+                    for i, r in enumerate([pl.ds(0, third), pl.ds(third, R - third)])]
+    gate_copies = copies(2, [(gain_h, gain), (wig_h, wig), (wfg_h, wfg)])
+    kv_copies = copies(3, [(wk, W.at[:, pl.ds(0, qk)]), (wv, W.at[:, pl.ds(o_v, vw)])])
+    small_copies = copies(4, [(bias_h, bias), (extra_h, extra), (taps_h, taps),
+                              (first_mem_h, first_mem), (first_norm_h, first_norm)])
+    rest_copies = copies(5, [(wq, W.at[:, pl.ds(o_q, qk)])] + [
+        (w, W.at[:, pl.ds(o_c + i * channels, channels)]) for i, w in enumerate((wcg, wcl, wcr))])
+    out_copies = copies(6, [(woc, WO.at[pl.ds(vw, channels), :]), (wom, WO.at[pl.ds(0, vw), :])])
+    for c in gate_copies + token_copies:
         c.start()
 
     def rows_of(block, first=0, n=None):
@@ -134,16 +133,7 @@
     def chip_rows(chip):
         return pl.ds(pl.multiple_of(chip * 2 * R, 16), 2 * R)
 
-    in_copies[0].wait()
-    in_copies[1].wait()
-    x = TK[...].astype(F32)
-    scale = lax.rsqrt(jnp.mean(x * x, axis=1, keepdims=True) + EPS)
-    XG[rows_of(tp), :] = (x * scale * gain[...]).astype(BF16)
-    pl.semaphore_wait(barrier, n_tp - 1 + n_earlier)
-    earlier(lambda k: pl.semaphore_signal(ent, inc=1, device_id=(sp - k, tp), device_id_type=MESH))
-
     pieces = gather_pieces(R)
-    third = R // 3
     sends = []
 
     def far_rows(chip, c, src_core):
@@ -154,14 +144,28 @@
 
     def y_piece(k, c, chip, to):
         src = XG.at[rows_of(tp, pieces[c][0], pieces[c][1]), :]
-        return remote(src, XG.at[far_rows(chip, c, core), :], ag_ys.at[k - 1, c], ag_yr.at[k - 1, c], to_tp=to)
-
-    for c in range(len(pieces)):
-        for k in range(1, n_y):
-            cp = y_piece(k, c, y, lax.rem(y + k, n_y) * 2 + core)
-            cp.start()
-            sends.append(cp)
-    own = remote(XG.at[rows_of(tp), :], XG.at[rows_of(tp), :], ag_d.at[0], ag_d.at[1], to_tp=partner)
+        return remote(src, XG.at[far_rows(chip, c, core), :], s_sem, ag_yr.at[k - 1, c], to_tp=to)
+
+    for c in gate_copies:
+        c.wait()
+    for c, (first, n) in enumerate(pieces):
+        if c < 2:
+            token_copies[c].wait()
+        x = TK[first:first + n, :].astype(F32)
+        scale = lax.rsqrt(jnp.mean(x * x, axis=1, keepdims=True) + EPS)
+        XG[rows_of(tp, first, n), :] = (x * scale * gain[...]).astype(BF16)
+        if c == 0:
+            pl.semaphore_wait(barrier, n_tp - 1 + n_earlier)
+        if c == 0 or c == len(pieces) - 1:
+            for cc in [0] if c == 0 else range(1, len(pieces)):
+                for k in range(1, n_y):
+                    cp = y_piece(k, cc, y, lax.rem(y + k, n_y) * 2 + core)
+                    cp.start()
+                    sends.append(cp)
+    for c in kv_copies + small_copies + rest_copies + out_copies:
+        c.start()
+    earlier(lambda k: pl.semaphore_signal(ent, inc=1, device_id=(sp - k, tp), device_id_type=MESH))
+    own = remote(XG.at[rows_of(tp), :], XG.at[rows_of(tp), :], s_sem, ag_d, to_tp=partner)
     own.start()
 
     def source(k):
@@ -172,14 +176,14 @@
             chip = source(k)
             y_piece(k, c, chip, partner).wait_recv()
             r = far_rows(chip, c, core)
-            cp = remote(XG.at[r, :], XG.at[r, :], ag_fs.at[k - 1, c], ag_fr.at[k - 1, c], to_tp=partner)
+            cp = remote(XG.at[r, :], XG.at[r, :], s_sem, ag_fr.at[k - 1, c], to_tp=partner)
             cp.start()
             sends.append(cp)
 
     def forwarded(c):
         for k in range(1, n_y):
             r = far_rows(source(k), c, 1 - core)
-            remote(XG.at[r, :], XG.at[r, :], ag_fs.at[k - 1, c], ag_fr.at[k - 1, c], to_tp=partner).wait_recv()
+            remote(XG.at[r, :], XG.at[r, :], s_sem, ag_fr.at[k - 1, c], to_tp=partner).wait_recv()
 
     kv_cols = [(0, o_g)]
     rest_cols = [(o_q, qk)] + [(o_c + i * channels, channels) for i in range(3)]
@@ -212,19 +216,15 @@
             for i in range(2):
                 G[to[i], :] = res[i * third:(i + 1) * third]
 
-    in_copies[2].wait()
-    in_copies[3].wait()
     W[:, o_g:o_g + 128] = jnp.concatenate(
         [wig[...].astype(F32), wfg[...].astype(F32), jnp.zeros((128 - 2 * n_heads, D), F32)],
         axis=0).T.astype(BF16)
-    for c in in_copies[4:]:
-        c.wait()
-    for c in w_copies[:2]:
+    for c in kv_copies:
         c.wait()
     own.wait_recv()
     project_local(kv_cols)
     local_gates()
-    for c in w_copies[2:6]:
+    for c in rest_copies:
         c.wait()
     project_local(rest_cols)
     for part in range(2):
@@ -237,8 +237,9 @@
     forward(3)
     forwarded(2)
     forwarded(3)
+    for c in small_copies:
+        c.wait()
     far_gates(2)
-    project_far(2, kv_cols)
 
     gt = G[...].T
     in_all, forget_all = gt[0:n_heads], gt[n_heads:2 * n_heads]
@@ -268,13 +269,15 @@
     s8 = lax.broadcasted_iota(jnp.int32, (8, 128), 0)
     pr = KEY_DIM // PARTS
 
+    project_far(2, kv_cols)
+
     def group_copies(k, h, p):
         to = sp - x_in + lax.rem(x_in + k, B)
         if p == 0:
             ref = SM.at[x_in, h]
         else:
             ref = ST.at[x_in, h, pl.ds((p - 1) * pr, pr), :]
-        return remote(ref, ref, xs_s.at[k - 1, h, p], xs_r.at[k - 1, h, p], to_sp=to)
+        return remote(ref, ref, s_sem, xs_r.at[k - 1, h, p], to_sp=to)
 
     def group_sends(fn):
         for k in range(1, B):
@@ -333,19 +336,19 @@
         else:
             rr = pl.ds((p - 1) * pr, pr)
             s, d = CO.at[h, rr, :], CI.at[h, rr, :]
-        return remote(s, d, ch_s.at[h, p], ch_r.at[h, p], to_sp=sp + B)
+        return remote(s, d, s_sem, ch_r.at[h, p], to_sp=sp + B)
 
     def chain_wait(h, p):
         if p == 0:
             d = CSI.at[h]
         else:
             d = CI.at[h, pl.ds((p - 1) * pr, pr), :]
-        remote(d, d, ch_s.at[h, p], ch_r.at[h, p], to_tp=partner).wait_recv()
+        remote(d, d, s_sem, ch_r.at[h, p], to_tp=partner).wait_recv()
 
     def group_wait(k, h, p):
         j = lax.rem(x_in + B - k, B)
         d = SM.at[j, h] if p == 0 else ST.at[j, h, pl.ds((p - 1) * pr, pr), :]
-        remote(d, d, xs_s.at[k - 1, h, p], xs_r.at[k - 1, h, p], to_tp=partner).wait_recv()
+        remote(d, d, s_sem, xs_r.at[k - 1, h, p], to_tp=partner).wait_recv()
 
     def relay(chained):
         for h in range(heads):
@@ -366,18 +369,17 @@
         last = min(MAX_SLOTS, A - 1)
         if s < last:
             pl.when(zg == s)(functools.partial(relay, s > 0))
-        if s == last:
-            if A - 1 > last:
-                pl.when((zg >= last) & (zg < A - 1))(functools.partial(relay, True))
-
-            @pl.when(zg == A - 1)
-            def _():
-                for h in range(heads):
-                    for p in range(PARTS + 1):
-                        for k in range(1, B):
-                            pl.when(k <= x_in)(functools.partial(group_wait, k, h, p))
-                        if A > 1:
-                            chain_wait(h, p)
+        if s == last and A - 1 > last:
+            pl.when((zg >= last) & (zg < A - 1))(functools.partial(relay, True))
+
+    def end_wait(h):
+        @pl.when(zg == A - 1)
+        def _():
+            for p in range(PARTS + 1):
+                for k in range(1, B):
+                    pl.when(k <= x_in)(functools.partial(group_wait, k, h, p))
+                if A > 1:
+                    chain_wait(h, p)
 
     rb = 256 if T % 256 == 0 else R
     q_scale = KEY_DIM ** -0.5
@@ -391,7 +393,7 @@
             RM[h] = jnp.broadcast_to(run[h:h + 1], (128, T)).T
 
     def halo_copy(to):
-        return remote(halo_out, halo_in, hl_s.at[0], hl_s.at[1], to_sp=to)
+        return remote(halo_out, halo_in, s_sem, hl_r, to_sp=to)
 
     def work_product():
         for r0 in range(0, T, rb):
@@ -442,35 +444,51 @@
     order = list(range(1, n_y)) + [0]
 
     def conv_copy(idx):
-        return remote(PSC.at[rows_of(2 * chips[idx] + 1 - core), :], DRC.at[idx], cd_s.at[idx], cd_r.at[idx],
+        return remote(PSC.at[rows_of(2 * chips[idx] + 1 - core), :], DRC.at[idx], s_sem, cd_r.at[idx],
                       to_tp=partner)
 
-    def conv_out():
-        w_copies[6].wait()
-        for idx in order:
+    def conv_out(which):
+        for idx in which:
             rr = chip_rows(chips[idx])
             for j in range(RS_CHUNKS):
                 cols = slice(j * cw, (j + 1) * cw)
                 PSC[rr, cols] = mm(CB[rr, :], WO[vw:, cols]).astype(BF16)
             conv_copy(idx).start()
 
+    early = EARLY * cw
+
+    def early_copy(k):
+        return remote(YC.at[k - 1], YCR.at[k - 1], s_sem, yc_r.at[k - 1],
+                      to_tp=lax.rem(y + k, n_y) * 2 + core)
+
+    def conv_early():
+        for k in range(1, n_y):
+            conv_copy(k).wait_recv()
+            mine = rows_of(2 * chips[k] + core)
+            s = PSC[mine, 0:early].astype(F32) + DRC[k, :, 0:early].astype(F32)
+            YC[k - 1] = s.astype(BF16)
+            early_copy(k).start()
+
     work_running_max()
     project_far(2, rest_cols)
-    slot(0)
     work_product()
-    for r0 in range(0, T, rb):
-        attend(0, r0)
-    slot(1)
-    for h in range(1, heads):
+    for h in range(heads):
         for r0 in range(0, T, rb):
             attend(h, r0)
+    slot(0)
+    slot(1)
     conv_finish()
+    for c in out_copies:
+        c.wait()
+    conv_out(order[:-1])
     slot(2)
-    conv_out()
+    conv_out(order[-1:])
+    conv_early()
     slot(3)
 
     sq = [None] * (T // rb)
     for h in range(heads):
+        end_wait(h)
         wts = weights(h, x_in)
         c_mem = joined(h, wts, 0, KEY_DIM)
         c_norm, cmax = wts[3], wts[4]
@@ -508,56 +526,81 @@
             at = b * (rb // 128) + i
             sq_out[at:at + 1, :] = row[:, i * 128:(i + 1) * 128]
     for k in range(1, n_tp):
-        cp = remote(sq_out, sq_in.at[k - 1], sq_s.at[k - 1], sq_r.at[k - 1], to_tp=lax.rem(tp + k, n_tp))
+        cp = remote(sq_out, sq_in.at[k - 1], s_sem, sq_r, to_tp=lax.rem(tp + k, n_tp))
         cp.start()
         sends.append(cp)
 
     def cols_of(j):
         return pl.ds(j * cw, cw)
 
-    def mem_copy(idx, j):
-        return remote(PSM.at[rows_of(2 * chips[idx] + 1 - core), cols_of(j)], DRM.at[idx, :, cols_of(j)],
-                      rd_s.at[idx, j], rd_r.at[idx, j], to_tp=partner)
-
-    w_copies[7].wait()
-    for idx in order:
+    parts = [(0, EARLY), (EARLY, RS_CHUNKS)]
+
+    def mem_copy(idx, q):
+        cols = pl.ds(parts[q][0] * cw, (parts[q][1] - parts[q][0]) * cw)
+        return remote(PSM.at[rows_of(2 * chips[idx] + 1 - core), cols], DRM.at[idx, :, cols],
+                      s_sem, rd_r.at[idx, q], to_tp=partner)
+
+    def mem_out(idx):
         rr = chip_rows(chips[idx])
-        for j in range(RS_CHUNKS):
-            cols = slice(j * cw, (j + 1) * cw)
-            PSM[rr, cols] = mm(MO[rr, :], WO[0:vw, cols]).astype(BF16)
-            mem_copy(idx, j).start()
-    for idx in order:
-        conv_copy(idx).wait_recv()
+        for q in range(2):
+            for j in range(*parts[q]):
+                cols = slice(j * cw, (j + 1) * cw)
+                PSM[rr, cols] = mm(MO[rr, :], WO[0:vw, cols]).astype(BF16)
+            mem_copy(idx, q).start()
+
+    def y_copy(k, j):
+        return remote(YS.at[k - 1, :, cols_of(j)], YR.at[k - 1, :, cols_of(j)], s_sem,
+                      ry_r.at[k - 1, j], to_tp=lax.rem(y + k, n_y) * 2 + core)
+
+    def mem_sum(idx, j):
+        cols = slice(j * cw, (j + 1) * cw)
+        mine = rows_of(2 * chips[idx] + core)
+        return PSM[mine, cols].astype(F32) + DRM[idx, :, cols].astype(F32)
+
+    for idx in order[:-1]:
+        mem_out(idx)
+    for k in range(1, n_y):
+        mem_copy(k, 0).wait_recv()
+        for j in range(EARLY):
+            YS[k - 1, :, j * cw:(j + 1) * cw] = mem_sum(k, j).astype(BF16)
+            y_copy(k, j).start()
+    mem_out(0)
 
     tot = sq_out[...]
+    remote(sq_in, sq_in, s_sem, sq_r, to_tp=partner).wait_recv()
     for k in range(1, n_tp):
-        remote(sq_out, sq_in.at[k - 1], sq_s.at[k - 1], sq_r.at[k - 1], to_tp=partner).wait_recv()
         tot = tot + sq_in[k - 1]
     r_scale = lax.rsqrt(tot / float(width) + EPS)
     for b in range(T // 128):
         RC[b * 128:(b + 1) * 128, :] = jnp.broadcast_to(r_scale[b:b + 1], (128, 128)).T
 
+    def row_scale(idx):
+        return jnp.concatenate([RC[rows_of(2 * chips[idx] + core), :]] * (cw // 128), axis=1)
+
     def chip_sum(idx, j):
         cols = slice(j * cw, (j + 1) * cw)
         mine = rows_of(2 * chips[idx] + core)
-        mem_copy(idx, j).wait_recv()
-        r = jnp.concatenate([RC[mine, :]] * (cw // 128), axis=1)
-        s = (PSM[mine, cols].astype(F32) + DRM[idx, :, cols].astype(F32)) * r
-        return s + (PSC[mine, cols].astype(F32) + DRC[idx, :, cols].astype(F32))
-
-    def y_copy(k, j):
-        return remote(YS.at[k - 1, :, cols_of(j)], YR.at[k - 1, :, cols_of(j)], ry_s.at[k - 1, j],
-                      ry_r.at[k - 1, j], to_tp=lax.rem(y + k, n_y) * 2 + core)
-
-    for j in range(RS_CHUNKS):
-        for k in range(1, n_y):
+        s = PSC[mine, cols].astype(F32) + DRC[idx, :, cols].astype(F32)
+        return s + mem_sum(idx, j) * row_scale(idx)
+
+    for k in range(1, n_y):
+        mem_copy(k, 1).wait_recv()
+        for j in range(EARLY, RS_CHUNKS):
             YS[k - 1, :, j * cw:(j + 1) * cw] = chip_sum(k, j).astype(BF16)
             y_copy(k, j).start()
+    conv_copy(0).wait_recv()
+    for q in range(2):
+        mem_copy(0, q).wait_recv()
+    for k in range(1, n_y):
+        early_copy(k).wait_recv()
     for j in range(RS_CHUNKS):
         s = chip_sum(0, j)
         for k in range(1, n_y):
             y_copy(k, j).wait_recv()
-            s = s + YR[k - 1, :, j * cw:(j + 1) * cw].astype(F32)
+            got = YR[k - 1, :, j * cw:(j + 1) * cw].astype(F32)
+            if j < EARLY:
+                got = got * row_scale(0) + YCR[k - 1, :, j * cw:(j + 1) * cw].astype(F32)
+            s = s + got
         out[:, j * cw:(j + 1) * cw] = s.astype(BF16)
 
     for cp in sends:
@@ -573,9 +616,10 @@
     pl.when(sp < n_sp - 1)(lambda: halo_copy(sp + 1).wait_send())
     for idx in range(n_y):
         conv_copy(idx).wait_send()
-        for j in range(RS_CHUNKS):
-            mem_copy(idx, j).wait_send()
+        for q in range(2):
+            mem_copy(idx, q).wait_send()
     for k in range(1, n_y):
+        early_copy(k).wait_send()
         for j in range(RS_CHUNKS):
             y_copy(k, j).wait_send()
 
@@ -600,6 +644,7 @@
     ny1 = n_y - 1
     np_ = len(gather_pieces(R))
     sq_rows = -(-T // 1024) * 8
+    early = EARLY * D // RS_CHUNKS
     return pl.pallas_call(
         functools.partial(kernel, n_sp, n_tp, heads, channels, n_heads * VALUE_DIM),
         out_shape=pltpu.VMEM((R, D), BF16),
@@ -619,12 +664,9 @@
             V((sq_rows, 128), F32), V((n_tp - 1, sq_rows, 128), F32), V((T, 128), F32),
             V((T, D), BF16), V((T, D), BF16), V((n_y, R, D), BF16), V((n_y, R, D), BF16),
             V((ny1, R, D), BF16), V((ny1, R, D), BF16),
-            dma((9,)), dma((8,)), dma((2,)), dma((ny1, np_)), dma((ny1, np_)),
-            dma((ny1, np_)), dma((ny1, np_)),
-            dma((B - 1, heads, PARTS + 1)), dma((B - 1, heads, PARTS + 1)),
-            dma((heads, PARTS + 1)), dma((heads, PARTS + 1)), dma((2,)),
-            dma((n_tp - 1,)), dma((n_tp - 1,)), dma((n_y,)), dma((n_y,)),
-            dma((n_y, RS_CHUNKS)), dma((n_y, RS_CHUNKS)), dma((ny1, RS_CHUNKS)), dma((ny1, RS_CHUNKS)),
+            V((ny1, R, early), BF16), V((ny1, R, early), BF16),
+            dma((7,)), dma, dma, dma((ny1, np_)), dma((ny1, np_)), dma((B - 1, heads, PARTS + 1)),
+            dma((heads, PARTS + 1)), dma, dma, dma((n_y,)), dma((n_y, 2)), dma((ny1, RS_CHUNKS)), dma((ny1,)),
             pltpu.SemaphoreType.REGULAR,
         ],
         compiler_params=pltpu.CompilerParams(

time: 62.1 us -> 57.4 us (0.924); the launches traced: 62 us -> 56.3 us
  Pallas kernels: 61.1 us -> 55.5 us
    pallas_call x1, Pallas kernels: 61.1 us -> 55.5 us  [per_device(): pl.pallas_call(functools.partial(kernel, n_sp, n_tp, heads, channels, n_h...]
where the time goes in v2:
time: 57.4 us; the launch traced here: 56.3 us
  Pallas kernels  55.5 us (97%)
  local copies, waits for them, and re-layouts  0.88 us (2%)
    pallas_call x1, Pallas kernels, per_device(): pl.pallas_call(functools.partial(kernel, n_sp, n_tp, heads, channels, n_h...  55.5 us

profile of v2, /device:TPU:0, one launch (start us, length us, event | category | flops | bytes accessed | tf_op | source)
XLA Modules:
  0.0 56.3 jit_solution(4790104718117457981)
XLA Ops:
  0.0 55.5 %layer.1 = bf16[192,2048]{1,0:T(8,128)(2,1)S(1)} custom-call(bf16[192,2048]{1,0:T(8,128)(2,1)} %tokens_h.1, f32[1,2048]{1,0:T(1,128)} %bitcast.6, bf16[2048,256]{1,0:T(8,128)(2,1)} %wk.1, bf16[2048,512]{1,0:T(8,128)(2,1)} %wv.1, bf16[2048,256]{1,0:T(8,128)(2,1)} %wq.1, bf16[2048,512]{1,0:T(8,128)(2,1)} %wcg.1, bf16[2048,512]{1,0:T(8,128)(2,1)} %wcl.1, ...), custom_call_target="tpu_custom_call" | custom-call | tf_op jit(solution)/shard_map/layer/pallas_call | solution.py:648
  55.5 0.9 %copy.19 = bf16[192,2048]{1,0:T(8,128)(2,1)} copy(bf16[192,2048]{1,0:T(8,128)(2,1)S(1)} %layer.1) | data formatting | bytes 1572864

commit v3 on v2

--- a/solution.py
+++ b/solution.py
@@ -56,7 +56,7 @@
     wom, woc, out,
     TK, gain, wig, wfg, bias, extra, taps, first_mem, first_norm,
     W, WO, XG, PJ, G, RM, NUM, DEN, MO, CB, PROD, halo_out, halo_in,
-    ST, SM, CO, CI, CSO, CSI, sq_out, sq_in, RC,
+    ST, SM, CO, CI, CSO, CSI, CW, sq_out, sq_in, RC,
     PSC, PSM, DRC, DRM, YS, YR, YC, YCR,
     i_sem, s_sem, ag_d, ag_yr, ag_fr, xs_r, ch_r, hl_r, sq_r, cd_r, rd_r, ry_r, yc_r, ent,
 ):
@@ -123,7 +123,7 @@
     rest_copies = copies(5, [(wq, W.at[:, pl.ds(o_q, qk)])] + [
         (w, W.at[:, pl.ds(o_c + i * channels, channels)]) for i, w in enumerate((wcg, wcl, wcr))])
     out_copies = copies(6, [(woc, WO.at[pl.ds(vw, channels), :]), (wom, WO.at[pl.ds(0, vw), :])])
-    for c in gate_copies + token_copies:
+    for c in token_copies[:1] + gate_copies + token_copies[1:]:
         c.start()
 
     def rows_of(block, first=0, n=None):
@@ -245,7 +245,6 @@
     in_all, forget_all = gt[0:n_heads], gt[n_heads:2 * n_heads]
     sub = lax.broadcasted_iota(jnp.int32, (n_heads, T), 0)
     sub8 = lax.broadcasted_iota(jnp.int32, (8, T), 0)
-    lane = lax.broadcasted_iota(jnp.int32, (8, T), 1)
     in_pre = jnp.zeros((8, T), F32)
     log_f = jnp.zeros((8, T), F32)
     for h in range(heads):
@@ -255,9 +254,24 @@
         row_f = jnp.minimum(row_f, 0.0) - jnp.log1p(jnp.exp(-jnp.abs(row_f))) + extra[h:h + 1, :]
         in_pre = jnp.where(sub8 == h, row_i, in_pre)
         log_f = jnp.where(sub8 == h, row_f, log_f)
-    cum = log_f
-    for d in scan_steps(T):
-        cum = cum + jnp.where(lane >= d, pltpu.roll(cum, d, 1), 0.0)
+    seg = T // 128
+    li = lax.broadcasted_iota(jnp.int32, (128, 128), 0)
+    lj = lax.broadcasted_iota(jnp.int32, (128, 128), 1)
+    tri = jnp.where(li <= lj, 1.0, 0.0).astype(BF16)
+    rows = jnp.concatenate([log_f[:, i * 128:(i + 1) * 128] for i in range(seg)], axis=0)
+    split, rem = [], rows
+    for _ in range(3):
+        split.append(rem.astype(BF16))
+        rem = rem - split[-1].astype(F32)
+    part = mm(jnp.concatenate(split, axis=0), tri)
+    n8 = 8 * seg
+    part = part[0:n8] + part[n8:2 * n8] + part[2 * n8:3 * n8]
+    ends = jnp.broadcast_to(part[:, 127:128], (n8, 128))
+    run_cum, base = [], jnp.zeros((8, 128), F32)
+    for i in range(seg):
+        run_cum.append(part[8 * i:8 * i + 8] + base)
+        base = base + ends[8 * i:8 * i + 8]
+    cum = jnp.concatenate(run_cum, axis=1)
     gap = in_pre - cum
     decay = cum[:, T - 1:T]
     gmax = jnp.max(gap, axis=1, keepdims=True)
@@ -321,13 +335,13 @@
             norm = norm + c_j[j] * ns[j]
         return c_c, c_j, valid, norm, top
 
-    def joined(h, wts, first, n):
-        c_c, c_j, valid = wts[:3]
+    def joined(h, c_c, c_j, valid, first, n):
         two = lambda v: jnp.concatenate([v] * (VALUE_DIM // 128), axis=1)
         r = slice(first, first + n)
         mem = two(c_c) * jnp.where(zg > 0, CI[h, r].astype(F32), first_mem[h, r])
         for j in range(B):
-            mem = mem + two(c_j[j]) * jnp.where(valid[j], ST[j, h, r].astype(F32), 0.0)
+            got = ST[j, h, r].astype(F32)
+            mem = mem + two(c_j[j]) * (got if valid is None else jnp.where(valid[j], got, 0.0))
         return mem
 
     def chain_copy(h, p):
@@ -350,27 +364,38 @@
         d = SM.at[j, h] if p == 0 else ST.at[j, h, pl.ds((p - 1) * pr, pr), :]
         remote(d, d, s_sem, xs_r.at[k - 1, h, p], to_tp=partner).wait_recv()
 
-    def relay(chained):
-        for h in range(heads):
-            wts = None
-            for p in range(PARTS + 1):
-                for k in range(1, B):
-                    group_wait(k, h, p)
-                if chained:
-                    chain_wait(h, p)
-                if p == 0:
-                    wts = weights(h, B)
-                    CSO[h] = jnp.where(s8 == 0, wts[3], wts[4])
-                else:
-                    CO[h, (p - 1) * pr:p * pr] = joined(h, wts, (p - 1) * pr, pr).astype(BF16)
-                chain_copy(h, p).start()
-
-    def slot(s):
-        last = min(MAX_SLOTS, A - 1)
-        if s < last:
-            pl.when(zg == s)(functools.partial(relay, s > 0))
-        if s == last and A - 1 > last:
-            pl.when((zg >= last) & (zg < A - 1))(functools.partial(relay, True))
+    def relay(chained, messages):
+        for h, p in messages:
+            for k in range(1, B):
+                group_wait(k, h, p)
+            if chained:
+                chain_wait(h, p)
+            if p == 0:
+                c_c, c_j, _, norm, top = weights(h, B)
+                CW[h, 0:1] = c_c
+                for j in range(B):
+                    CW[h, j + 1:j + 2] = c_j[j]
+                CSO[h] = jnp.where(s8 == 0, norm, top)
+            else:
+                c_j = [CW[h, j + 1:j + 2] for j in range(B)]
+                mem = joined(h, CW[h, 0:1], c_j, None, (p - 1) * pr, pr)
+                CO[h, (p - 1) * pr:p * pr] = mem.astype(BF16)
+            chain_copy(h, p).start()
+
+    messages = [(h, p) for h in range(heads) for p in range(PARTS + 1)]
+    last = min(MAX_SLOTS, A - 1)
+    left = [list(messages) for _ in range(last)]
+
+    def pass_on(z, n):
+        if z < last and left[z]:
+            now, left[z] = left[z][:n], left[z][n:]
+            pl.when(zg == z)(functools.partial(relay, z > 0, now))
+
+    def pass_rest():
+        for z in range(last):
+            pass_on(z, len(messages))
+        if A - 1 > last:
+            pl.when((zg >= last) & (zg < A - 1))(functools.partial(relay, True, messages))
 
     def end_wait(h):
         @pl.when(zg == A - 1)
@@ -386,9 +411,17 @@
     shifted = gap + math.log(q_scale)
 
     def work_running_max():
-        run = gap
-        for d in scan_steps(T):
-            run = jnp.maximum(run, jnp.where(lane >= d, pltpu.roll(run, d, 1), run))
+        run = jnp.concatenate([gap[:, i * 128:(i + 1) * 128] for i in range(seg)], axis=0)
+        lane8 = lax.broadcasted_iota(jnp.int32, (n8, 128), 1)
+        for d in scan_steps(128):
+            run = jnp.maximum(run, jnp.where(lane8 >= d, pltpu.roll(run, d, 1), run))
+        ends = jnp.broadcast_to(run[:, 127:128], (n8, 128))
+        runs = [run[0:8]]
+        ends_top = ends[0:8]
+        for i in range(1, seg):
+            runs.append(jnp.maximum(run[8 * i:8 * i + 8], ends_top))
+            ends_top = jnp.maximum(ends_top, ends[8 * i:8 * i + 8])
+        run = jnp.concatenate(runs, axis=1)
         for h in range(heads):
             RM[h] = jnp.broadcast_to(run[h:h + 1], (128, T)).T
 
@@ -447,12 +480,12 @@
         return remote(PSC.at[rows_of(2 * chips[idx] + 1 - core), :], DRC.at[idx], s_sem, cd_r.at[idx],
                       to_tp=partner)
 
-    def conv_out(which):
-        for idx in which:
-            rr = chip_rows(chips[idx])
-            for j in range(RS_CHUNKS):
-                cols = slice(j * cw, (j + 1) * cw)
-                PSC[rr, cols] = mm(CB[rr, :], WO[vw:, cols]).astype(BF16)
+    def conv_out(idx, q):
+        rr = chip_rows(chips[idx])
+        for j in range(q * RS_CHUNKS // 2, (q + 1) * RS_CHUNKS // 2):
+            cols = slice(j * cw, (j + 1) * cw)
+            PSC[rr, cols] = mm(CB[rr, :], WO[vw:, cols]).astype(BF16)
+        if q == 1:
             conv_copy(idx).start()
 
     early = EARLY * cw
@@ -475,22 +508,42 @@
     for h in range(heads):
         for r0 in range(0, T, rb):
             attend(h, r0)
-    slot(0)
-    slot(1)
+    pass_on(0, 10)
+    pass_on(1, 10)
     conv_finish()
     for c in out_copies:
         c.wait()
-    conv_out(order[:-1])
-    slot(2)
-    conv_out(order[-1:])
+    for idx in order[:-1]:
+        for q in range(2):
+            conv_out(idx, q)
+    pass_on(2, 10)
+    for idx in order[-1:]:
+        for q in range(2):
+            conv_out(idx, q)
     conv_early()
-    slot(3)
-
-    sq = [None] * (T // rb)
+    pass_rest()
+
+    parts = [(0, EARLY), (EARLY, RS_CHUNKS // 2), (RS_CHUNKS // 2, RS_CHUNKS)]
+    per_chip = -(-2 * R // 128)
+
+    def mem_copy(idx, q):
+        cols = pl.ds(parts[q][0] * cw, (parts[q][1] - parts[q][0]) * cw)
+        return remote(PSM.at[rows_of(2 * chips[idx] + 1 - core), cols], DRM.at[idx, :, cols],
+                      s_sem, rd_r.at[idx, q], to_tp=partner)
+
+    def mem_out(idx, q):
+        rr = chip_rows(chips[idx])
+        for j in range(*parts[q]):
+            cols = slice(j * cw, (j + 1) * cw)
+            PSM[rr, cols] = mm(MO[rr, :], WO[0:vw, cols]).astype(BF16)
+        mem_copy(idx, q).start()
+
+    sq_out[...] = jnp.zeros_like(sq_out)
+    sq = [None] * n_y
     for h in range(heads):
         end_wait(h)
         wts = weights(h, x_in)
-        c_mem = joined(h, wts, 0, KEY_DIM)
+        c_mem = joined(h, *wts[:3], 0, KEY_DIM)
         c_norm, cmax = wts[3], wts[4]
         hi = c_mem.astype(BF16)
         lo = (c_mem - hi.astype(F32)).astype(BF16)
@@ -499,32 +552,33 @@
         n_hi = n_col.astype(BF16)
         n_lo = (n_col - n_hi.astype(F32)).astype(BF16)
         n_two = jnp.concatenate([n_hi, n_lo], axis=0)
-        for b, r0 in enumerate(range(0, T, rb)):
-            e = r0 + rb
-            q = PJ[r0:e, o_q + h * KEY_DIM:o_q + (h + 1) * KEY_DIM]
+        for idx in order:
+            rr = chip_rows(chips[idx])
+            q = PJ[rr, o_q + h * KEY_DIM:o_q + (h + 1) * KEY_DIM]
             qq = jnp.concatenate([q, q], axis=1)
             fm = mm(qq, two)
             fn = mm(qq, n_two)
-            m0 = RM[h, r0:e, :]
+            m0 = RM[h, rr, :]
             m = jnp.maximum(m0, cmax)
             k0 = jnp.exp(m0 - m)
             k1 = jnp.exp(cmax - m) * q_scale
-            den = k0 * DEN[h, r0:e, :] + k1 * fn
+            den = k0 * DEN[h, rr, :] + k1 * fn
             inv = 1.0 / jnp.maximum(jnp.abs(den), 1.0)
             k0, k1 = k0 * inv, k1 * inv
             cols = slice(h * VALUE_DIM, (h + 1) * VALUE_DIM)
-            mo = (jnp.concatenate([k0, k0], axis=1) * NUM[r0:e, cols]
+            mo = (jnp.concatenate([k0, k0], axis=1) * NUM[rr, cols]
                   + jnp.concatenate([k1, k1], axis=1) * fm)
-            MO[r0:e, cols] = mo.astype(BF16)
+            MO[rr, cols] = mo.astype(BF16)
             s2 = mo * mo
             s2 = s2[:, 0:128] + s2[:, 128:256]
-            sq[b] = s2 if sq[b] is None else sq[b] + s2
-    sq_out[...] = jnp.zeros_like(sq_out)
-    for b in range(T // rb):
-        row = jnp.sum(sq[b].T, axis=0, keepdims=True)
-        for i in range(rb // 128):
-            at = b * (rb // 128) + i
-            sq_out[at:at + 1, :] = row[:, i * 128:(i + 1) * 128]
+            sq[idx] = s2 if sq[idx] is None else sq[idx] + s2
+            if h == heads - 1 and idx > 0:
+                mem_out(idx, 0)
+    for idx in range(n_y):
+        for i in range(per_chip):
+            n = min(128, 2 * R - i * 128)
+            row = jnp.sum(sq[idx][i * 128:i * 128 + n].T, axis=0, keepdims=True)
+            sq_out[pl.ds(chips[idx] * per_chip + i, 1), 0:n] = row
     for k in range(1, n_tp):
         cp = remote(sq_out, sq_in.at[k - 1], s_sem, sq_r, to_tp=lax.rem(tp + k, n_tp))
         cp.start()
@@ -533,21 +587,6 @@
     def cols_of(j):
         return pl.ds(j * cw, cw)
 
-    parts = [(0, EARLY), (EARLY, RS_CHUNKS)]
-
-    def mem_copy(idx, q):
-        cols = pl.ds(parts[q][0] * cw, (parts[q][1] - parts[q][0]) * cw)
-        return remote(PSM.at[rows_of(2 * chips[idx] + 1 - core), cols], DRM.at[idx, :, cols],
-                      s_sem, rd_r.at[idx, q], to_tp=partner)
-
-    def mem_out(idx):
-        rr = chip_rows(chips[idx])
-        for q in range(2):
-            for j in range(*parts[q]):
-                cols = slice(j * cw, (j + 1) * cw)
-                PSM[rr, cols] = mm(MO[rr, :], WO[0:vw, cols]).astype(BF16)
-            mem_copy(idx, q).start()
-
     def y_copy(k, j):
         return remote(YS.at[k - 1, :, cols_of(j)], YR.at[k - 1, :, cols_of(j)], s_sem,
                       ry_r.at[k - 1, j], to_tp=lax.rem(y + k, n_y) * 2 + core)
@@ -558,21 +597,27 @@
         return PSM[mine, cols].astype(F32) + DRM[idx, :, cols].astype(F32)
 
     for idx in order[:-1]:
-        mem_out(idx)
+        mem_out(idx, 1)
     for k in range(1, n_y):
         mem_copy(k, 0).wait_recv()
         for j in range(EARLY):
             YS[k - 1, :, j * cw:(j + 1) * cw] = mem_sum(k, j).astype(BF16)
             y_copy(k, j).start()
-    mem_out(0)
+    for idx in order[:-1]:
+        mem_out(idx, 2)
+    for q in range(3):
+        mem_out(0, q)
 
     tot = sq_out[...]
     remote(sq_in, sq_in, s_sem, sq_r, to_tp=partner).wait_recv()
     for k in range(1, n_tp):
         tot = tot + sq_in[k - 1]
     r_scale = lax.rsqrt(tot / float(width) + EPS)
-    for b in range(T // 128):
-        RC[b * 128:(b + 1) * 128, :] = jnp.broadcast_to(r_scale[b:b + 1], (128, 128)).T
+    for c in range(n_y):
+        for i in range(per_chip):
+            n = min(128, 2 * R - i * 128)
+            at = c * 2 * R + i * 128
+            RC[at:at + n, :] = jnp.broadcast_to(r_scale[c * per_chip + i:c * per_chip + i + 1, 0:n], (128, n)).T
 
     def row_scale(idx):
         return jnp.concatenate([RC[rows_of(2 * chips[idx] + core), :]] * (cw // 128), axis=1)
@@ -584,12 +629,13 @@
         return s + mem_sum(idx, j) * row_scale(idx)
 
     for k in range(1, n_y):
-        mem_copy(k, 1).wait_recv()
+        for q in range(1, 3):
+            mem_copy(k, q).wait_recv()
         for j in range(EARLY, RS_CHUNKS):
             YS[k - 1, :, j * cw:(j + 1) * cw] = chip_sum(k, j).astype(BF16)
             y_copy(k, j).start()
     conv_copy(0).wait_recv()
-    for q in range(2):
+    for q in range(3):
         mem_copy(0, q).wait_recv()
     for k in range(1, n_y):
         early_copy(k).wait_recv()
@@ -616,7 +662,7 @@
     pl.when(sp < n_sp - 1)(lambda: halo_copy(sp + 1).wait_send())
     for idx in range(n_y):
         conv_copy(idx).wait_send()
-        for q in range(2):
+        for q in range(3):
             mem_copy(idx, q).wait_send()
     for k in range(1, n_y):
         early_copy(k).wait_send()
@@ -643,7 +689,7 @@
     V, dma = pltpu.VMEM, pltpu.SemaphoreType.DMA
     ny1 = n_y - 1
     np_ = len(gather_pieces(R))
-    sq_rows = -(-T // 1024) * 8
+    sq_rows = -(-(n_y * -(-2 * R // 128)) // 8) * 8
     early = EARLY * D // RS_CHUNKS
     return pl.pallas_call(
         functools.partial(kernel, n_sp, n_tp, heads, channels, n_heads * VALUE_DIM),
@@ -660,13 +706,13 @@
             V((16, channels), BF16), V((16, channels), BF16),
             V((B, heads, KEY_DIM, VALUE_DIM), BF16), V((B, heads, 8, 128), F32),
             V((heads, KEY_DIM, VALUE_DIM), BF16), V((heads, KEY_DIM, VALUE_DIM), BF16),
-            V((heads, 8, 128), F32), V((heads, 8, 128), F32),
+            V((heads, 8, 128), F32), V((heads, 8, 128), F32), V((heads, 8 * -(-(B + 1) // 8), 128), F32),
             V((sq_rows, 128), F32), V((n_tp - 1, sq_rows, 128), F32), V((T, 128), F32),
             V((T, D), BF16), V((T, D), BF16), V((n_y, R, D), BF16), V((n_y, R, D), BF16),
             V((ny1, R, D), BF16), V((ny1, R, D), BF16),
             V((ny1, R, early), BF16), V((ny1, R, early), BF16),
             dma((7,)), dma, dma, dma((ny1, np_)), dma((ny1, np_)), dma((B - 1, heads, PARTS + 1)),
-            dma((heads, PARTS + 1)), dma, dma, dma((n_y,)), dma((n_y, 2)), dma((ny1, RS_CHUNKS)), dma((ny1,)),
+            dma((heads, PARTS + 1)), dma, dma, dma((n_y,)), dma((n_y, 3)), dma((ny1, RS_CHUNKS)), dma((ny1,)),
             pltpu.SemaphoreType.REGULAR,
         ],
         compiler_params=pltpu.CompilerParams(

time: 57.4 us -> 57 us (level)
  no operation moved by 1% of the time
where the time goes in v3:
time: 57 us; the launch traced here: 56 us
  Pallas kernels  55.1 us (97%)
  local copies, waits for them, and re-layouts  0.88 us (2%)
    pallas_call x1, Pallas kernels, per_device(): pl.pallas_call(functools.partial(kernel, n_sp, n_tp, heads, channels, n_h...  55.1 us

profile of v3, /device:TPU:0, one launch (start us, length us, event | category | flops | bytes accessed | tf_op | source)
XLA Modules:
  0.0 56.0 jit_solution(7881499697289548666)
XLA Ops:
  0.0 55.1 %layer.1 = bf16[192,2048]{1,0:T(8,128)(2,1)S(1)} custom-call(bf16[192,2048]{1,0:T(8,128)(2,1)} %tokens_h.1, f32[1,2048]{1,0:T(1,128)} %bitcast.6, bf16[2048,256]{1,0:T(8,128)(2,1)} %wk.1, bf16[2048,512]{1,0:T(8,128)(2,1)} %wv.1, bf16[2048,256]{1,0:T(8,128)(2,1)} %wq.1, bf16[2048,512]{1,0:T(8,128)(2,1)} %wcg.1, bf16[2048,512]{1,0:T(8,128)(2,1)} %wcl.1, ...), custom_call_target="tpu_custom_call" | custom-call | tf_op jit(solution)/shard_map/layer/pallas_call | solution.py:694
  55.1 0.9 %copy.19 = bf16[192,2048]{1,0:T(8,128)(2,1)} copy(bf16[192,2048]{1,0:T(8,128)(2,1)S(1)} %layer.1) | data formatting | bytes 1572864

commit v4 on v3

--- a/solution.py
+++ b/solution.py
@@ -605,7 +605,7 @@
             y_copy(k, j).start()
     for idx in order[:-1]:
         mem_out(idx, 2)
-    for q in range(3):
+    for q in range(2):
         mem_out(0, q)
 
     tot = sq_out[...]
@@ -634,6 +634,7 @@
         for j in range(EARLY, RS_CHUNKS):
             YS[k - 1, :, j * cw:(j + 1) * cw] = chip_sum(k, j).astype(BF16)
             y_copy(k, j).start()
+    mem_out(0, 2)
     conv_copy(0).wait_recv()
     for q in range(3):
         mem_copy(0, q).wait_recv()

time: 57 us -> 56.8 us (level)
  no operation moved by 1% of the time
where the time goes in v4:
time: 56.8 us; the launch traced here: 55.8 us
  Pallas kernels  54.9 us (97%)
  local copies, waits for them, and re-layouts  0.88 us (2%)
    pallas_call x1, Pallas kernels, per_device(): pl.pallas_call(functools.partial(kernel, n_sp, n_tp, heads, channels, n_h...  54.9 us

profile of v4, /device:TPU:0, one launch (start us, length us, event | category | flops | bytes accessed | tf_op | source)
XLA Modules:
  0.0 55.8 jit_solution(9325674812181998496)
XLA Ops:
  0.0 54.9 %layer.1 = bf16[192,2048]{1,0:T(8,128)(2,1)S(1)} custom-call(bf16[192,2048]{1,0:T(8,128)(2,1)} %tokens_h.1, f32[1,2048]{1,0:T(1,128)} %bitcast.6, bf16[2048,256]{1,0:T(8,128)(2,1)} %wk.1, bf16[2048,512]{1,0:T(8,128)(2,1)} %wv.1, bf16[2048,256]{1,0:T(8,128)(2,1)} %wq.1, bf16[2048,512]{1,0:T(8,128)(2,1)} %wcg.1, bf16[2048,512]{1,0:T(8,128)(2,1)} %wcl.1, ...), custom_call_target="tpu_custom_call" | custom-call | tf_op jit(solution)/shard_map/layer/pallas_call | solution.py:695
  54.9 0.9 %copy.19 = bf16[192,2048]{1,0:T(8,128)(2,1)} copy(bf16[192,2048]{1,0:T(8,128)(2,1)S(1)} %layer.1) | data formatting | bytes 1572864
